TPU v7x, 512 devices: a 4x2x32 block of a 4x8x32 slice. The times are simulated.
512 devices in a mesh: grp: 2 (over y), tp: 32 (over z), dp: 8 (over x, core).
Axes of the slice: x: 4, y: 2, z: 32, core: 2. Of those that a mesh axis runs over, the one named last changes fastest.
The devices are a block of a 4x8x32 slice.
Arguments:
- tokens: bfloat16 [256, 4096], P('grp', 'dp'), parts along dimension 0, may hold values from -6 to 6
- norm_gain: float32 [2, 4096], P(None, 'dp'), may hold values from 0.1 to 1.9
- w_query: bfloat16 [2, 4096, 4096], P(None, 'dp', 'tp'), may hold values from -0.09375 to 0.09375
- w_key: bfloat16 [2, 4096, 4096], P(None, 'dp', 'tp'), may hold values from -0.09375 to 0.09375
- w_value: bfloat16 [2, 4096, 4096], P(None, 'dp', 'tp'), may hold values from -0.09375 to 0.09375
- w_outgate: bfloat16 [2, 4096, 4096], P(None, 'dp', 'tp'), may hold values from -0.09375 to 0.09375
- gate_weight: bfloat16 [2, 32, 384, 2], P(None, 'tp'), may hold values from -0.3125 to 0.3125
- forget_bias: float32 [2, 32], P(None, 'tp'), may hold values from -2 to 4
- w_mix: bfloat16 [2, 4096, 4096], P(None, 'tp', 'dp'), may hold values from -0.09375 to 0.09375
- memory: float32 [2, 256, 32, 128, 128], P(None, ('grp', 'dp'), 'tp'), parts along dimension 1, may hold values from -3 to 3
- normalizer: float32 [2, 256, 32, 128], P(None, ('grp', 'dp'), 'tp'), parts along dimension 1, may hold values from -3 to 3
- stabilizer: float32 [2, 256, 32], P(None, ('grp', 'dp'), 'tp'), parts along dimension 1, may hold values from -4 to 4
Outputs:
- result: bfloat16 [256, 4096], P('grp', 'dp'), parts along dimension 0
- new_memory: float32 [2, 256, 32, 128, 128], P(None, ('grp', 'dp'), 'tp'), parts along dimension 1
- new_normalizer: float32 [2, 256, 32, 128], P(None, ('grp', 'dp'), 'tp'), parts along dimension 1
- new_stabilizer: float32 [2, 256, 32], P(None, ('grp', 'dp'), 'tp'), parts along dimension 1
There are 2 independent parts, one for each index of `grp`. A program takes and returns all parts, laid end to end along the dimension named above; an argument that names none is the same for every part. Nothing has to cross between parts.
All inputs are finite; a program needn't handle non-finite values.
Results may differ from a plain program's by a relative error of at most 0.018.
Values may be sent and summed in bfloat16 or wider, within the bound.
A program may use at most 64 MiB of HBM per device.

v0:
```python
import jax
import jax.numpy as jnp
from jax import lax
from jax.sharding import PartitionSpec as P

D = 4096
DK = 128
BLOCKS = 2


EPS = 1e-06


def split_up(array, dim, count):
    before, after = (array.shape[:dim], array.shape[dim + 1 :])
    return jnp.moveaxis(array.reshape(*before, count, -1, *after), dim, 0)


def summed_on_arrival(array, axis, dim):
    blocks = split_up(array, dim, lax.axis_size(axis))
    arrived = lax.all_to_all(blocks, axis, split_axis=0, concat_axis=0, tiled=True)
    return arrived.sum(axis=0)


def joined_along(blocks, dim):
    lengths = list(blocks.shape[1:])
    lengths[dim] *= blocks.shape[0]
    return jnp.moveaxis(blocks, 0, dim).reshape(lengths)


def copy_for_each(array, axis):
    copies = jnp.broadcast_to(array, (lax.axis_size(axis), *array.shape))
    return lax.all_to_all(copies, axis, split_axis=0, concat_axis=0, tiled=True)


def gather_directly(array, axis, dim):
    return joined_along(copy_for_each(array, axis), dim)


def summed_on_arrival_2(array, axis, dim):
    blocks = split_up(array, dim, lax.axis_size(axis))
    arrived = lax.all_to_all(blocks, axis, split_axis=0, concat_axis=0, tiled=True)
    return arrived.astype(jnp.float32).sum(axis=0)


def shards(
    tokens,
    norm_gain,
    w_query,
    w_key,
    w_value,
    w_outgate,
    gate_weight,
    forget_bias,
    w_mix,
    memory,
    normalizer,
    stabilizer,
):
    x = tokens
    seq_own = memory.shape[1]
    heads_own = memory.shape[2]
    mems, norms, stabs = ([], [], [])
    for blk in range(BLOCKS):
        xf = x.astype(jnp.float32)
        squares = jnp.sum(xf * xf, axis=-1)
        scaled_in = (xf * norm_gain[blk]).astype(jnp.bfloat16)
        terms = tuple(
            (
                jnp.dot(scaled_in, weight[blk], preferred_element_type=jnp.float32)
                for weight in (w_query, w_key, w_value, w_outgate)
            )
        )
        packed = jax.tree.map(lambda part: summed_on_arrival(part, "dp", 0), terms + (squares,))
        summed = packed[:4]
        own_squares = packed[4]
        scale = lax.rsqrt(own_squares / D + EPS)
        projs = [
            (scale[:, None] * part)
            .astype(jnp.bfloat16)
            .astype(jnp.float32)
            .reshape(seq_own, heads_own, DK)
            for part in summed
        ]
        query, key, value, outgate = projs
        joined = jnp.concatenate([query, key, value], axis=-1)
        pre = jnp.einsum(
            "shc,hcg->shg",
            joined,
            gate_weight[blk].astype(jnp.float32),
            precision=lax.Precision.HIGHEST,
        )
        log_input = pre[..., 0]
        log_forget = jax.nn.log_sigmoid(pre[..., 1] + forget_bias[blk])
        stab = stabilizer[blk]
        new_stab = jnp.maximum(log_forget + stab, log_input)
        keep = jnp.exp(log_forget + stab - new_stab)
        admit = jnp.exp(log_input - new_stab)
        scaled_key = key * DK ** (-0.5)
        new_mem = (
            keep[..., None, None] * memory[blk]
            + admit[..., None, None] * scaled_key[..., :, None] * value[..., None, :]
        )
        new_norm = keep[..., None] * normalizer[blk] + admit[..., None] * scaled_key
        numer = jnp.einsum("shd,shde->she", query, new_mem, precision=lax.Precision.HIGHEST)
        denom = jnp.maximum(jnp.abs(jnp.sum(query * new_norm, axis=-1)), 1.0)
        readout = numer / denom[..., None]
        gated = (
            (readout * jax.nn.sigmoid(outgate))
            .reshape(seq_own, heads_own * DK)
            .astype(jnp.bfloat16)
        )
        mix_weight = w_mix[blk]
        partial_mix = jnp.dot(
            gather_directly(gated, "dp", 0), mix_weight, preferred_element_type=jnp.float32
        )
        mine = summed_on_arrival_2(partial_mix.astype(jnp.bfloat16), "tp", 0)
        row_count = mine.shape[0]
        own_rows = lax.dynamic_slice_in_dim(xf, lax.axis_index("tp") * row_count, row_count, 0)
        updated = (own_rows + mine).astype(jnp.bfloat16)
        x = gather_directly(updated, "tp", 0)
        mems.append(new_mem)
        norms.append(new_norm)
        stabs.append(new_stab)
    return (x, jnp.stack(mems, axis=0), jnp.stack(norms, axis=0), jnp.stack(stabs, axis=0))


def solution(mesh):
    in_specs = (
        P("grp", "dp"),
        P(None, "dp"),
        P(None, "dp", "tp"),
        P(None, "dp", "tp"),
        P(None, "dp", "tp"),
        P(None, "dp", "tp"),
        P(None, "tp", None, None),
        P(None, "tp"),
        P(None, "tp", "dp"),
        P(None, ("grp", "dp"), "tp", None, None),
        P(None, ("grp", "dp"), "tp", None),
        P(None, ("grp", "dp"), "tp"),
    )
    out_specs = (
        P("grp", "dp"),
        P(None, ("grp", "dp"), "tp", None, None),
        P(None, ("grp", "dp"), "tp", None),
        P(None, ("grp", "dp"), "tp"),
    )
    return jax.shard_map(shards, mesh=mesh, in_specs=in_specs, out_specs=out_specs, check_vma=False)
```

profile of v0, /device:TPU:40, one launch (start us, length us, event | category | flops | bytes accessed | tf_op | source)
XLA Modules:
  0.0 297.8 jit_solution(17828496100304087356)
XLA Ops:
  3.8 4.6 %all-to-all-start = ((f32[8,1,16]{2,1,0:T(1,128)}), f32[8,1,16]{2,1,0:T(1,128)S(1)}, u32[]{:S(2)}, u32[]{:S(2)}) async-start(f32[8,1,16]{2,1,0:T(1,128)} %bitcast), calls=%async_computation | async-start | bytes 8192 | tf_op jit(solution)/shard_map/all_to_all | solution.py:21
  8.4 1.7 fusion.26
  10.1 1.7 fusion.28
  11.9 1.7 fusion.30
  13.6 4.8 %all-to-all-start.3 = ((f32[8,16,128]{2,1,0:T(8,128)}), f32[8,16,128]{2,1,0:T(8,128)S(1)}, u32[]{:S(2)}, u32[]{:S(2)}) async-start(f32[8,16,128]{2,1,0:T(8,128)} %fusion.28), calls=%async_computation.3 | async-start | bytes 131072 | tf_op jit(solution)/shard_map/all_to_all | solution.py:21
  18.4 1.7 fusion.32
  20.1 3.9 %all-to-all-done.3 = f32[8,16,128]{2,1,0:T(8,128)S(1)} async-done(((f32[8,16,128]{2,1,0:T(8,128)}), f32[8,16,128]{2,1,0:T(8,128)S(1)}, u32[]{:S(2)}, u32[]{:S(2)}) %all-to-all-start.3) | async-done | bytes 65568 | tf_op jit(solution)/shard_map/all_to_all | solution.py:21
  24.0 3.6 %all-to-all-start.1 = ((f32[8,16,128]{2,1,0:T(8,128)}), f32[8,16,128]{2,1,0:T(8,128)S(1)}, u32[]{:S(2)}, u32[]{:S(2)}) async-start(f32[8,16,128]{2,1,0:T(8,128)} %fusion.32), calls=%async_computation.1 | async-start | bytes 131072 | tf_op jit(solution)/shard_map/all_to_all | solution.py:21
  29.0 4.0 %all-to-all-done.1 = f32[8,16,128]{2,1,0:T(8,128)S(1)} async-done(((f32[8,16,128]{2,1,0:T(8,128)}), f32[8,16,128]{2,1,0:T(8,128)S(1)}, u32[]{:S(2)}, u32[]{:S(2)}) %all-to-all-start.1) | async-done | bytes 65568 | tf_op jit(solution)/shard_map/all_to_all | solution.py:21
  33.0 3.6 %all-to-all-start.2 = ((f32[8,16,128]{2,1,0:T(8,128)}), f32[8,16,128]{2,1,0:T(8,128)S(1)}, u32[]{:S(2)}, u32[]{:S(2)}) async-start(f32[8,16,128]{2,1,0:T(8,128)} %fusion.30), calls=%async_computation.2 | async-start | bytes 131072 | tf_op jit(solution)/shard_map/all_to_all | solution.py:21
  36.6 5.3 %all-to-all-done.2 = f32[8,16,128]{2,1,0:T(8,128)S(1)} async-done(((f32[8,16,128]{2,1,0:T(8,128)}), f32[8,16,128]{2,1,0:T(8,128)S(1)}, u32[]{:S(2)}, u32[]{:S(2)}) %all-to-all-start.2) | async-done | bytes 65568 | tf_op jit(solution)/shard_map/all_to_all | solution.py:21
  41.9 3.6 %all-to-all-start.4 = ((f32[8,16,128]{2,1,0:T(8,128)}), f32[8,16,128]{2,1,0:T(8,128)S(1)}, u32[]{:S(2)}, u32[]{:S(2)}) async-start(f32[8,16,128]{2,1,0:T(8,128)} %fusion.26), calls=%async_computation.4 | async-start | bytes 131072 | tf_op jit(solution)/shard_map/all_to_all | solution.py:21
  48.6 2.3 all-to-all-done.4
  51.0 7.9 %all_to_all.88 = bf16[8,16,128]{2,1,0:T(8,128)(2,1)S(1)} all-to-all(bf16[8,16,128]{2,1,0:T(8,128)(2,1)S(1)} %broadcast_in_dim.8), channel_id=1, replica_groups=mesh['grp'=2,'tp'=32,'dp'=8] {'dp'}, dimensions={0} | all-to-all | bytes 65536 | tf_op jit(solution)/shard_map/all_to_all | solution.py:33
  59.7 45.8 %all-to-all-start.6 = ((bf16[32,4,512]{2,1,0:T(4,128)(2,1)}), bf16[32,4,512]{2,1,0:T(4,128)(2,1)S(1)}, u32[]{:S(2)}, u32[]{:S(2)}) async-start(bf16[32,4,512]{2,1,0:T(4,128)(2,1)} %reshape.1119), calls=%async_computation.6 | async-start | bytes 262144 | tf_op jit(solution)/shard_map/all_to_all | solution.py:42
  105.6 30.7 %all-to-all-done.6 = bf16[32,4,512]{2,1,0:T(4,128)(2,1)S(1)} async-done(((bf16[32,4,512]{2,1,0:T(4,128)(2,1)}), bf16[32,4,512]{2,1,0:T(4,128)(2,1)S(1)}, u32[]{:S(2)}, u32[]{:S(2)}) %all-to-all-start.6) | async-done | bytes 131104 | tf_op jit(solution)/shard_map/all_to_all | solution.py:42
  136.4 33.2 %all_to_all.89 = bf16[32,4,512]{2,1,0:T(4,128)(2,1)S(1)} all-to-all(bf16[32,4,512]{2,1,0:T(4,128)(2,1)S(1)} %broadcast_in_dim.9), channel_id=1, replica_groups=mesh['grp'=2,'tp'=32,'dp'=8] {'tp'}, dimensions={0} | all-to-all | bytes 262144 | tf_op jit(solution)/shard_map/all_to_all | solution.py:33
  171.2 4.1 %all-to-all-start.8 = ((f32[8,1,16]{2,1,0:T(1,128)}), f32[8,1,16]{2,1,0:T(1,128)}, u32[]{:S(2)}, u32[]{:S(2)}) async-start(f32[8,1,16]{2,1,0:T(1,128)} %bitcast.36), calls=%async_computation.8 | async-start | bytes 8192 | tf_op jit(solution)/shard_map/all_to_all | solution.py:21
  176.9 3.4 %all-to-all-done.8 = f32[8,1,16]{2,1,0:T(1,128)} async-done(((f32[8,1,16]{2,1,0:T(1,128)}), f32[8,1,16]{2,1,0:T(1,128)}, u32[]{:S(2)}, u32[]{:S(2)}) %all-to-all-start.8) | async-done | bytes 544 | tf_op jit(solution)/shard_map/all_to_all | solution.py:21
  180.4 3.6 %all-to-all-start.11 = ((f32[8,16,128]{2,1,0:T(8,128)}), f32[8,16,128]{2,1,0:T(8,128)S(1)}, u32[]{:S(2)}, u32[]{:S(2)}) async-start(f32[8,16,128]{2,1,0:T(8,128)} %fusion.19), calls=%async_computation.11 | async-start | bytes 131072 | tf_op jit(solution)/shard_map/all_to_all | solution.py:21
  184.8 4.6 %all-to-all-done.11 = f32[8,16,128]{2,1,0:T(8,128)S(1)} async-done(((f32[8,16,128]{2,1,0:T(8,128)}), f32[8,16,128]{2,1,0:T(8,128)S(1)}, u32[]{:S(2)}, u32[]{:S(2)}) %all-to-all-start.11) | async-done | bytes 65568 | tf_op jit(solution)/shard_map/all_to_all | solution.py:21
  189.3 3.6 %all-to-all-start.9 = ((f32[8,16,128]{2,1,0:T(8,128)}), f32[8,16,128]{2,1,0:T(8,128)S(1)}, u32[]{:S(2)}, u32[]{:S(2)}) async-start(f32[8,16,128]{2,1,0:T(8,128)} %fusion.23), calls=%async_computation.9 | async-start | bytes 131072 | tf_op jit(solution)/shard_map/all_to_all | solution.py:21
  192.9 1.7 fusion.21
  195.3 3.0 all-to-all-done.9
  198.3 3.6 %all-to-all-start.10 = ((f32[8,16,128]{2,1,0:T(8,128)}), f32[8,16,128]{2,1,0:T(8,128)S(1)}, u32[]{:S(2)}, u32[]{:S(2)}) async-start(f32[8,16,128]{2,1,0:T(8,128)} %fusion.21), calls=%async_computation.10 | async-start | bytes 131072 | tf_op jit(solution)/shard_map/all_to_all | solution.py:21
  201.9 5.3 %all-to-all-done.10 = f32[8,16,128]{2,1,0:T(8,128)S(1)} async-done(((f32[8,16,128]{2,1,0:T(8,128)}), f32[8,16,128]{2,1,0:T(8,128)S(1)}, u32[]{:S(2)}, u32[]{:S(2)}) %all-to-all-start.10) | async-done | bytes 65568 | tf_op jit(solution)/shard_map/all_to_all | solution.py:21
  207.2 3.6 %all-to-all-start.12 = ((f32[8,16,128]{2,1,0:T(8,128)}), f32[8,16,128]{2,1,0:T(8,128)S(1)}, u32[]{:S(2)}, u32[]{:S(2)}) async-start(f32[8,16,128]{2,1,0:T(8,128)} %fusion.17), calls=%async_computation.12 | async-start | bytes 131072 | tf_op jit(solution)/shard_map/all_to_all | solution.py:21
  216.3 9.8 %all_to_all.90 = bf16[8,16,128]{2,1,0:T(8,128)(2,1)S(1)} all-to-all(bf16[8,16,128]{2,1,0:T(8,128)(2,1)S(1)} %broadcast_in_dim.10), channel_id=1, replica_groups=mesh['grp'=2,'tp'=32,'dp'=8] {'dp'}, dimensions={0} | all-to-all | bytes 65536 | tf_op jit(solution)/shard_map/all_to_all | solution.py:33
  227.0 4.8 %all-to-all-start.14 = ((bf16[32,4,512]{2,1,0:T(4,128)(2,1)}), bf16[32,4,512]{2,1,0:T(4,128)(2,1)S(1)}, u32[]{:S(2)}, u32[]{:S(2)}) async-start(bf16[32,4,512]{2,1,0:T(4,128)(2,1)} %reshape.1123), calls=%async_computation.14 | async-start | bytes 262144 | tf_op jit(solution)/shard_map/all_to_all | solution.py:42
  233.8 29.0 %all-to-all-done.14 = bf16[32,4,512]{2,1,0:T(4,128)(2,1)S(1)} async-done(((bf16[32,4,512]{2,1,0:T(4,128)(2,1)}), bf16[32,4,512]{2,1,0:T(4,128)(2,1)S(1)}, u32[]{:S(2)}, u32[]{:S(2)}) %all-to-all-start.14) | async-done | bytes 131104 | tf_op jit(solution)/shard_map/all_to_all | solution.py:42
  263.6 4.8 %all-to-all-start.15 = ((bf16[32,4,512]{2,1,0:T(4,128)(2,1)}), bf16[32,4,512]{2,1,0:T(4,128)(2,1)S(1)}, u32[]{:S(2)}, u32[]{:S(2)}) async-start(bf16[32,4,512]{2,1,0:T(4,128)(2,1)} %broadcast_in_dim.11), calls=%async_computation.15 | async-start | bytes 262144 | tf_op jit(solution)/shard_map/all_to_all | solution.py:33
  271.4 25.7 %all-to-all-done.15 = bf16[32,4,512]{2,1,0:T(4,128)(2,1)S(1)} async-done(((bf16[32,4,512]{2,1,0:T(4,128)(2,1)}), bf16[32,4,512]{2,1,0:T(4,128)(2,1)S(1)}, u32[]{:S(2)}, u32[]{:S(2)}) %all-to-all-start.15) | async-done | bytes 131104 | tf_op jit(solution)/shard_map/all_to_all | solution.py:33
  (116 shorter events, 26.4 us)
Async XLA Ops:
  0.6 45.0 %copy-start.23 = (bf16[2,1,384,2]{2,3,1,0:T(2,128)(2,1)S(1)}, bf16[2,1,384,2]{2,3,1,0:T(2,128)(2,1)}, u32[]{:S(2)}) copy-start(bf16[2,1,384,2]{2,3,1,0:T(2,128)(2,1)} %param.18) | copy-start | bytes 9220
  0.6 45.1 %copy-start.13 = (f32[2,16,1]{1,2,0:T(1,128)S(1)}, f32[2,16,1]{1,2,0:T(1,128)}, u32[]{:S(2)}) copy-start(f32[2,16,1]{1,2,0:T(1,128)} %param.23) | copy-start | bytes 388
  0.7 46.7 %copy-start.9 = (f32[2,16,1,128]{3,2,1,0:T(1,128)S(1)}, f32[2,16,1,128]{3,2,1,0:T(1,128)}, u32[]{:S(2)}) copy-start(f32[2,16,1,128]{3,2,1,0:T(1,128)} %param.22) | copy-start | bytes 49156
  0.7 47.1 %copy-start = (f32[2,16,1,128,128]{4,3,2,1,0:T(8,128)S(1)}, f32[2,16,1,128,128]{4,3,2,1,0:T(8,128)}, u32[]{:S(2)}) copy-start(f32[2,16,1,128,128]{4,3,2,1,0:T(8,128)} %param.21) | copy-start | bytes 6291460
  0.7 58.2 %copy-start.5 = (bf16[2,128,512]{2,1,0:T(8,128)(2,1)S(1)}, bf16[2,128,512]{2,1,0:T(8,128)(2,1)}, u32[]{:S(2)}) copy-start(bf16[2,128,512]{2,1,0:T(8,128)(2,1)} %param.20) | copy-start | bytes 786436
  3.8 9.8 %all-to-all-start = ((f32[8,1,16]{2,1,0:T(1,128)}), f32[8,1,16]{2,1,0:T(1,128)S(1)}, u32[]{:S(2)}, u32[]{:S(2)}) async-start(f32[8,1,16]{2,1,0:T(1,128)} %bitcast), calls=%async_computation | async-start | bytes 8192 | tf_op jit(solution)/shard_map/all_to_all | solution.py:21
  10.1 95.4 %copy-start.1 = (bf16[128,512]{1,0:T(8,128)(2,1)S(1)}, bf16[128,512]{1,0:T(8,128)(2,1)}, u32[]{:S(2)}) copy-start(bf16[128,512]{1,0:T(8,128)(2,1)} %param.12) | copy-start | bytes 393220
  13.6 10.4 %all-to-all-start.3 = ((f32[8,16,128]{2,1,0:T(8,128)}), f32[8,16,128]{2,1,0:T(8,128)S(1)}, u32[]{:S(2)}, u32[]{:S(2)}) async-start(f32[8,16,128]{2,1,0:T(8,128)} %fusion.28), calls=%async_computation.3 | async-start | bytes 131072 | tf_op jit(solution)/shard_map/all_to_all | solution.py:21
  24.0 9.0 %all-to-all-start.1 = ((f32[8,16,128]{2,1,0:T(8,128)}), f32[8,16,128]{2,1,0:T(8,128)S(1)}, u32[]{:S(2)}, u32[]{:S(2)}) async-start(f32[8,16,128]{2,1,0:T(8,128)} %fusion.32), calls=%async_computation.1 | async-start | bytes 131072 | tf_op jit(solution)/shard_map/all_to_all | solution.py:21
  33.0 9.0 %all-to-all-start.2 = ((f32[8,16,128]{2,1,0:T(8,128)}), f32[8,16,128]{2,1,0:T(8,128)S(1)}, u32[]{:S(2)}, u32[]{:S(2)}) async-start(f32[8,16,128]{2,1,0:T(8,128)} %fusion.30), calls=%async_computation.2 | async-start | bytes 131072 | tf_op jit(solution)/shard_map/all_to_all | solution.py:21
  36.5 22.3 %copy-start.15 = (f32[16]{0:T(128)}, f32[16]{0:T(128)S(1)}, u32[]{:S(2)}) copy-start(f32[16]{0:T(128)S(1)} %add_rsqrt_fusion.1) | copy-start | bytes 196
  36.6 138.8 %copy-start.2 = (bf16[2,512,128]{2,1,0:T(8,128)(2,1)S(1)}, bf16[2,512,128]{2,1,0:T(8,128)(2,1)}, u32[]{:S(2)}) copy-start(bf16[2,512,128]{2,1,0:T(8,128)(2,1)} %param.17) | copy-start | bytes 786436
  41.9 8.9 %all-to-all-start.4 = ((f32[8,16,128]{2,1,0:T(8,128)}), f32[8,16,128]{2,1,0:T(8,128)S(1)}, u32[]{:S(2)}, u32[]{:S(2)}) async-start(f32[8,16,128]{2,1,0:T(8,128)} %fusion.26), calls=%async_computation.4 | async-start | bytes 131072 | tf_op jit(solution)/shard_map/all_to_all | solution.py:21
  45.5 130.6 %copy-start.3 = (bf16[2,512,128]{2,1,0:T(8,128)(2,1)S(1)}, bf16[2,512,128]{2,1,0:T(8,128)(2,1)}, u32[]{:S(2)}) copy-start(bf16[2,512,128]{2,1,0:T(8,128)(2,1)} %param.16) | copy-start | bytes 786436
  47.8 136.1 %copy-start.4 = (bf16[2,512,128]{2,1,0:T(8,128)(2,1)S(1)}, bf16[2,512,128]{2,1,0:T(8,128)(2,1)}, u32[]{:S(2)}) copy-start(bf16[2,512,128]{2,1,0:T(8,128)(2,1)} %param.14) | copy-start | bytes 786436
  59.7 76.6 %all-to-all-start.6 = ((bf16[32,4,512]{2,1,0:T(4,128)(2,1)}), bf16[32,4,512]{2,1,0:T(4,128)(2,1)S(1)}, u32[]{:S(2)}, u32[]{:S(2)}) async-start(bf16[32,4,512]{2,1,0:T(4,128)(2,1)} %reshape.1119), calls=%async_computation.6 | async-start | bytes 262144 | tf_op jit(solution)/shard_map/all_to_all | solution.py:42
  169.7 56.5 %copy-start.6 = (bf16[2,128,512]{2,1,0:T(8,128)(2,1)S(1)}, bf16[2,128,512]{2,1,0:T(8,128)(2,1)}, u32[]{:S(2)}) copy-start(bf16[2,128,512]{2,1,0:T(8,128)(2,1)} %param.20) | copy-start | bytes 786436
  171.2 9.2 %all-to-all-start.8 = ((f32[8,1,16]{2,1,0:T(1,128)}), f32[8,1,16]{2,1,0:T(1,128)}, u32[]{:S(2)}, u32[]{:S(2)}) async-start(f32[8,1,16]{2,1,0:T(1,128)} %bitcast.36), calls=%async_computation.8 | async-start | bytes 8192 | tf_op jit(solution)/shard_map/all_to_all | solution.py:21
  176.9 54.9 %copy-start.12 = (f32[16,1,2]{0,2,1:T(2,128)S(1)}, f32[16,1,2]{0,2,1:T(2,128)}, u32[]{:S(2)}) copy-start(f32[16,1,2]{0,2,1:T(2,128)} %copy-done.11) | copy-start | bytes 388
  176.9 54.9 %copy-start.14 = (f32[2,16,1]{1,2,0:T(1,128)S(1)}, f32[2,16,1]{1,2,0:T(1,128)}, u32[]{:S(2)}) copy-start(f32[2,16,1]{1,2,0:T(1,128)} %param.23) | copy-start | bytes 388
  180.4 9.0 %all-to-all-start.11 = ((f32[8,16,128]{2,1,0:T(8,128)}), f32[8,16,128]{2,1,0:T(8,128)S(1)}, u32[]{:S(2)}, u32[]{:S(2)}) async-start(f32[8,16,128]{2,1,0:T(8,128)} %fusion.19), calls=%async_computation.11 | async-start | bytes 131072 | tf_op jit(solution)/shard_map/all_to_all | solution.py:21
  184.7 83.6 %copy-start.10 = (f32[2,16,1,128]{3,2,1,0:T(1,128)S(1)}, f32[2,16,1,128]{3,2,1,0:T(1,128)}, u32[]{:S(2)}) copy-start(f32[2,16,1,128]{3,2,1,0:T(1,128)} %param.22) | copy-start | bytes 49156
  184.7 83.6 %copy-start.16 = (f32[16]{0:T(128)S(1)}, f32[16]{0:T(128)}, u32[]{:S(2)}) copy-start(f32[16]{0:T(128)} %copy-done.15) | copy-start | bytes 196
  184.8 83.6 %copy-start.20 = (f32[16]{0:T(128)S(1)}, f32[16]{0:T(128)}, u32[]{:S(2)}) copy-start(f32[16]{0:T(128)} %copy-done.19) | copy-start | bytes 196
  184.8 83.6 %copy-start.22 = (f32[16]{0:T(128)S(1)}, f32[16]{0:T(128)}, u32[]{:S(2)}) copy-start(f32[16]{0:T(128)} %copy-done.21) | copy-start | bytes 196
  189.3 9.0 %all-to-all-start.9 = ((f32[8,16,128]{2,1,0:T(8,128)}), f32[8,16,128]{2,1,0:T(8,128)S(1)}, u32[]{:S(2)}, u32[]{:S(2)}) async-start(f32[8,16,128]{2,1,0:T(8,128)} %fusion.23), calls=%async_computation.9 | async-start | bytes 131072 | tf_op jit(solution)/shard_map/all_to_all | solution.py:21
  192.9 76.3 %copy-start.8 = (f32[16,128]{1,0:T(8,128)S(1)}, f32[16,128]{1,0:T(8,128)}, u32[]{:S(2)}) copy-start(f32[16,128]{1,0:T(8,128)} %copy-done.7) | copy-start | bytes 24580
  192.9 76.3 %copy-start.18 = (f32[16]{0:T(128)S(1)}, f32[16]{0:T(128)}, u32[]{:S(2)}) copy-start(f32[16]{0:T(128)} %copy-done.17) | copy-start | bytes 196
  198.3 9.0 %all-to-all-start.10 = ((f32[8,16,128]{2,1,0:T(8,128)}), f32[8,16,128]{2,1,0:T(8,128)S(1)}, u32[]{:S(2)}, u32[]{:S(2)}) async-start(f32[8,16,128]{2,1,0:T(8,128)} %fusion.21), calls=%async_computation.10 | async-start | bytes 131072 | tf_op jit(solution)/shard_map/all_to_all | solution.py:21
  207.2 9.0 %all-to-all-start.12 = ((f32[8,16,128]{2,1,0:T(8,128)}), f32[8,16,128]{2,1,0:T(8,128)S(1)}, u32[]{:S(2)}, u32[]{:S(2)}) async-start(f32[8,16,128]{2,1,0:T(8,128)} %fusion.17), calls=%async_computation.12 | async-start | bytes 131072 | tf_op jit(solution)/shard_map/all_to_all | solution.py:21
  227.0 35.8 %all-to-all-start.14 = ((bf16[32,4,512]{2,1,0:T(4,128)(2,1)}), bf16[32,4,512]{2,1,0:T(4,128)(2,1)S(1)}, u32[]{:S(2)}, u32[]{:S(2)}) async-start(bf16[32,4,512]{2,1,0:T(4,128)(2,1)} %reshape.1123), calls=%async_computation.14 | async-start | bytes 262144 | tf_op jit(solution)/shard_map/all_to_all | solution.py:42
  263.6 33.5 %all-to-all-start.15 = ((bf16[32,4,512]{2,1,0:T(4,128)(2,1)}), bf16[32,4,512]{2,1,0:T(4,128)(2,1)S(1)}, u32[]{:S(2)}, u32[]{:S(2)}) async-start(bf16[32,4,512]{2,1,0:T(4,128)(2,1)} %broadcast_in_dim.11), calls=%async_computation.15 | async-start | bytes 262144 | tf_op jit(solution)/shard_map/all_to_all | solution.py:33
  (5 other events, 16.3 us)
where the time goes:
time: 299 us; the launch traced here: 298 us
  waiting for transfers between devices  117 us (39%)
  starting transfers between devices  93.6 us (31%)
  blocking collectives  50.9 us (17%)
  matrix products  13.8 us (5%)
  other arithmetic  13.7 us (5%)
  local copies, waits for them, and re-layouts  7.45 us (2%)
    all_to_all x2, waiting for transfers between devices, summed_on_arrival_2(): lax.all_to_all(blocks, axis, split_axis=0, concat_axis=0, tiled=True)  59.7 us
    all_to_all x3, blocking collectives, copy_for_each(): return lax.all_to_all(copies, axis, split_axis=0, concat_axis=0, tiled=True)  50.9 us
    all_to_all x2, starting transfers between devices, summed_on_arrival_2(): lax.all_to_all(blocks, axis, split_axis=0, concat_axis=0, tiled=True)  50.5 us
    all_to_all x10, starting transfers between devices, summed_on_arrival(): lax.all_to_all(blocks, axis, split_axis=0, concat_axis=0, tiled=True)  38.3 us
    all_to_all x10, waiting for transfers between devices, summed_on_arrival(): lax.all_to_all(blocks, axis, split_axis=0, concat_axis=0, tiled=True)  31.8 us
    all_to_all x1, waiting for transfers between devices, copy_for_each(): return lax.all_to_all(copies, axis, split_axis=0, concat_axis=0, tiled=True)  25.7 us
    dot_general x8, matrix products, shards(): jnp.dot(scaled_in, weight[blk], preferred_element_type=jnp.float32)  11 us
  transfers between devices with their start and end apart: 13, of which 12 were waited for; matrix products, arithmetic and copies ran while one was open for 9% of the time, Pallas kernels for 0%

commit v1 on v0

v1 whole, which is shorter than its diff:
```python
import functools

import jax
import jax.numpy as jnp
from jax import lax
from jax.experimental import pallas as pl
from jax.experimental.pallas import tpu as pltpu
from jax.sharding import PartitionSpec as P

EPS = 1e-06
MESH = pl.DeviceIdType.MESH
NEAR = 8
EXTRA = 128
ANY = pl.BlockSpec(memory_space=pl.ANY)
VM = pl.BlockSpec(memory_space=pltpu.VMEM)


def ahead_first(count):
    return sorted(range(1, count), key=lambda k: -min(k, count - k))


def step_kernel(
    n_dp, n_tp, dims,
    tokens, gain, wq, wk, wv, wo, gate_w, bias, wmix, memory, norm, stab,
    x_out, vec_out,
    xbuf, wbuf, mixbuf, membuf, part, send1, recv1, gath, mixpart, send3, recv3, far,
    load_sem, s1, r1, s2, r2, s3, r3, s4, r4, s5, r5,
):
    blocks, rows, feats, dk, model = dims
    cols = 4 * dk
    dp, tp = lax.axis_index("dp"), lax.axis_index("tp")
    n_far = n_tp // NEAR
    group, j = tp // NEAR, lax.rem(tp, NEAR)

    def at_dp(k):
        return {"dp": lax.rem(dp + k, n_dp)}

    def at_near(k):
        return {"tp": group * NEAR + lax.rem(j + k, NEAR)}

    def at_tp(k):
        return {"tp": lax.rem(tp + k + n_tp, n_tp)}

    window = sorted(range(-(NEAR // 2) + 1, NEAR // 2 + 1), key=lambda k: -abs(k))
    window = [k for k in window if k]

    barrier = pltpu.get_barrier_semaphore()
    peers = [at_tp(NEAR * k) for k in ahead_first(n_far)]
    peers += [at_near(k) for k in ahead_first(NEAR)]
    peers += [at_tp(k) for h in range(1, NEAR // 2 + 1) for k in (h, -h)]
    peers += [at_dp(k) for k in ahead_first(n_dp)]
    for peer in peers:
        pl.semaphore_signal(barrier, inc=1, device_id=peer, device_id_type=MESH)

    loads = []

    def load(src, dst):
        copy = pltpu.make_async_copy(src, dst, load_sem.at[len(loads)])
        copy.start()
        loads.append(copy)
        return copy

    w_loads, mix_loads, mem_loads = [], [], []
    for b in range(blocks):
        w_loads.append(
            [load(w.at[b], wbuf.at[b, :, pl.ds(i * dk, dk)]) for i, w in enumerate((wq, wk, wv, wo))]
        )
        mem_loads.append(load(memory.at[b, :, 0], membuf.at[b]))
        mix_loads.append(load(wmix.at[b], mixbuf.at[b]))

    pl.semaphore_wait(barrier, len(peers))

    def rows_of(block):
        return pl.ds(pl.multiple_of(block * rows, rows), rows)

    sent = []

    def push(src, dst, send, recv, peer):
        copy = pltpu.make_async_remote_copy(
            src_ref=src, dst_ref=dst, send_sem=send, recv_sem=recv,
            device_id=peer, device_id_type=MESH,
        )
        copy.start()
        sent.append(copy)
        return copy

    for b in range(blocks):
        x_now = tokens if b == 0 else xbuf.at[b - 1]
        xf = x_now[...].astype(jnp.float32)
        scaled_in = (xf * gain[b : b + 1, :]).astype(jnp.bfloat16)
        squares = jnp.sum(xf * xf, axis=-1, keepdims=True)
        high = squares.astype(jnp.bfloat16).astype(jnp.float32)
        lane = lax.broadcasted_iota(jnp.int32, (xf.shape[0], EXTRA), 1)
        tail = jnp.where(lane == 0, high, jnp.where(lane == 1, squares - high, 0.0))
        send1[b, :, cols:] = tail.astype(jnp.bfloat16)
        for copy in w_loads[b]:
            copy.wait()
        prod = jnp.dot(scaled_in, wbuf[b], preferred_element_type=jnp.float32)
        part[...] = prod
        send1[b, :, :cols] = prod.astype(jnp.bfloat16)
        copies = [
            push(send1.at[b, rows_of(lax.rem(dp + k, n_dp))], recv1.at[b, k - 1],
                 s1.at[b, k - 1], r1.at[b, k - 1], at_dp(k))
            for k in ahead_first(n_dp)
        ]
        total = part[rows_of(dp), :]
        own_tail = send1[b, rows_of(dp), cols:].astype(jnp.float32)
        for copy in copies:
            copy.wait_recv()
        for k in range(1, n_dp):
            total = total + recv1[b, k - 1, :, :cols].astype(jnp.float32)
            own_tail = own_tail + recv1[b, k - 1, :, cols:].astype(jnp.float32)
        all_squares = jnp.sum(own_tail, axis=-1, keepdims=True)
        scale = lax.rsqrt(all_squares / model + EPS)
        proj = (scale * total).astype(jnp.bfloat16)
        query, key, value, outgate = (
            proj[:, i * dk : (i + 1) * dk].astype(jnp.float32) for i in range(4)
        )
        pre = jnp.dot(proj[:, : 3 * dk], gate_w[b, 0], preferred_element_type=jnp.float32)
        log_input = pre[:, 0:1]
        shifted = pre[:, 1:2] + bias[b : b + 1, 0:1]
        log_forget = jnp.minimum(shifted, 0.0) - jnp.log1p(jnp.exp(-jnp.abs(shifted)))
        old = stab[b]
        new_stab = jnp.maximum(log_forget + old, log_input)
        keep = jnp.exp(log_forget + old - new_stab)
        admit = jnp.exp(log_input - new_stab)
        scaled_key = key * dk ** (-0.5)
        admitted = admit * scaled_key
        new_norm = keep * norm[b, :, 0] + admitted
        mem_loads[b].wait()
        query_t = query.T
        recalled = jnp.concatenate(
            [
                jnp.sum(query_t[:, s : s + 1] * membuf[b, s], axis=0, keepdims=True)
                for s in range(rows)
            ],
            axis=0,
        )
        match = jnp.sum(query * admitted, axis=-1, keepdims=True)
        numer = keep * recalled + match * value
        denom = jnp.maximum(jnp.abs(jnp.sum(query * new_norm, axis=-1, keepdims=True)), 1.0)
        gated = numer / denom * jax.nn.sigmoid(outgate)
        gath[b, rows_of(dp), :] = gated.astype(jnp.bfloat16)
        copies = [
            push(gath.at[b, rows_of(dp)], gath.at[b, rows_of(dp)],
                 s2.at[b, k - 1], r2.at[b, k - 1], at_dp(k))
            for k in ahead_first(n_dp)
        ]
        vec_out[b, 0] = jnp.broadcast_to(keep, (rows, dk))
        vec_out[b, 1] = admitted
        vec_out[b, 2] = value
        vec_out[b, 3] = new_norm
        vec_out[b, 4] = jnp.broadcast_to(new_stab, (rows, dk))
        mix_loads[b].wait()
        for copy in copies:
            copy.wait_recv()
        prod = jnp.dot(gath[b], mixbuf[b], preferred_element_type=jnp.float32)
        mixpart[...] = prod
        send3[b] = prod.astype(jnp.bfloat16)
        copies = [
            push(send3.at[b, rows_of(lax.rem(j + k, NEAR))], recv3.at[b, k - 1],
                 s3.at[b, k - 1], r3.at[b, k - 1], at_near(k))
            for k in ahead_first(NEAR)
        ]
        total = mixpart[rows_of(j), :]
        for copy in copies:
            copy.wait_recv()
        for k in range(1, NEAR):
            total = total + recv3[b, k - 1].astype(jnp.float32)
        far[b, group] = total.astype(jnp.bfloat16)
        copies = [
            push(far.at[b, group], far.at[b, group], s4.at[b, k - 1], r4.at[b, k - 1], at_tp(NEAR * k))
            for k in ahead_first(n_far)
        ]
        total = x_now[rows_of(j), :].astype(jnp.float32)
        for copy in copies:
            copy.wait_recv()
        mixed = far[b, 0].astype(jnp.float32)
        for k in range(1, n_far):
            mixed = mixed + far[b, k].astype(jnp.float32)
        xbuf[b, rows_of(j), :] = (total + mixed).astype(jnp.bfloat16)
        copies = [
            push(xbuf.at[b, rows_of(j)], xbuf.at[b, rows_of(j)], s5.at[b, i], r5.at[b, i], at_tp(k))
            for i, k in enumerate(window)
        ]
        for copy in copies:
            copy.wait_recv()
    x_out[...] = xbuf[blocks - 1]
    for copy in sent:
        copy.wait_send()


def finish_kernel(rows, x, vec, memory, x_out, mem_out, norm_out, stab_out):
    admitted_t = vec[0, 1].T
    for s in range(rows):
        mem_out[0, s, 0] = (
            vec[0, 0, s : s + 1, :] * memory[0, s, 0]
            + admitted_t[:, s : s + 1] * vec[0, 2, s : s + 1, :]
        )
    norm_out[0, :, 0] = vec[0, 3]
    stab_out[0] = vec[0, 4, :, 0:1]
    x_out[...] = x[...]


def shards(n_dp, n_tp, *args):
    tokens, gain, wq, wk, wv, wo, gate_w, bias, wmix, memory, norm, stab = args
    blocks, rows, _, dk, _ = memory.shape
    seqs, feats = tokens.shape
    n_far = n_tp // NEAR
    dims = (blocks, rows, feats, dk, feats * n_dp)
    bf, f32 = jnp.bfloat16, jnp.float32
    dma = pltpu.SemaphoreType.DMA
    x, vec = pl.pallas_call(
        functools.partial(step_kernel, n_dp, n_tp, dims),
        out_shape=(
            jax.ShapeDtypeStruct((seqs, feats), bf),
            jax.ShapeDtypeStruct((blocks, 5, rows, dk), f32),
        ),
        in_specs=[VM, VM, ANY, ANY, ANY, ANY, VM, VM, ANY, ANY, VM, VM],
        out_specs=(VM, VM),
        scratch_shapes=[
            pltpu.VMEM((blocks, seqs, feats), bf),
            pltpu.VMEM((blocks, feats, 4 * dk), bf),
            pltpu.VMEM((blocks, dk, feats), bf),
            pltpu.VMEM((blocks, rows, dk, dk), f32),
            pltpu.VMEM((seqs, 4 * dk), f32),
            pltpu.VMEM((blocks, seqs, 4 * dk + EXTRA), bf),
            pltpu.VMEM((blocks, n_dp - 1, rows, 4 * dk + EXTRA), bf),
            pltpu.VMEM((blocks, seqs, dk), bf),
            pltpu.VMEM((seqs, feats), f32),
            pltpu.VMEM((blocks, seqs, feats), bf),
            pltpu.VMEM((blocks, NEAR - 1, rows, feats), bf),
            pltpu.VMEM((blocks, n_far, rows, feats), bf),
            dma((blocks * 6,)),
            dma((blocks, n_dp - 1)),
            dma((blocks, n_dp - 1)),
            dma((blocks, n_dp - 1)),
            dma((blocks, n_dp - 1)),
            dma((blocks, NEAR - 1)),
            dma((blocks, NEAR - 1)),
            dma((blocks, n_far - 1)),
            dma((blocks, n_far - 1)),
            dma((blocks, NEAR - 1)),
            dma((blocks, NEAR - 1)),
        ],
        compiler_params=pltpu.CompilerParams(collective_id=0, has_side_effects=True),
        name="two_cells",
    )(*args)
    return tuple(
        pl.pallas_call(
            functools.partial(finish_kernel, rows),
            grid=(blocks,),
            out_shape=(
                jax.ShapeDtypeStruct((seqs, feats), bf),
                jax.ShapeDtypeStruct(memory.shape, f32),
                jax.ShapeDtypeStruct(norm.shape, f32),
                jax.ShapeDtypeStruct(stab.shape, f32),
            ),
            in_specs=[
                pl.BlockSpec((seqs, feats), lambda b: (0, 0)),
                pl.BlockSpec((1, 5, rows, dk), lambda b: (b, 0, 0, 0)),
                pl.BlockSpec((1, rows, 1, dk, dk), lambda b: (b, 0, 0, 0, 0)),
            ],
            out_specs=(
                pl.BlockSpec((seqs, feats), lambda b: (0, 0)),
                pl.BlockSpec((1, rows, 1, dk, dk), lambda b: (b, 0, 0, 0, 0)),
                pl.BlockSpec((1, rows, 1, dk), lambda b: (b, 0, 0, 0)),
                pl.BlockSpec((1, rows, 1), lambda b: (b, 0, 0)),
            ),
            name="finish",
        )(x, vec, memory)
    )


def solution(mesh):
    in_specs = (
        P("grp", "dp"),
        P(None, "dp"),
        P(None, "dp", "tp"),
        P(None, "dp", "tp"),
        P(None, "dp", "tp"),
        P(None, "dp", "tp"),
        P(None, "tp", None, None),
        P(None, "tp"),
        P(None, "tp", "dp"),
        P(None, ("grp", "dp"), "tp", None, None),
        P(None, ("grp", "dp"), "tp", None),
        P(None, ("grp", "dp"), "tp"),
    )
    out_specs = (
        P("grp", "dp"),
        P(None, ("grp", "dp"), "tp", None, None),
        P(None, ("grp", "dp"), "tp", None),
        P(None, ("grp", "dp"), "tp"),
    )
    body = functools.partial(shards, mesh.shape["dp"], mesh.shape["tp"])
    return jax.shard_map(body, mesh=mesh, in_specs=in_specs, out_specs=out_specs, check_vma=False)
```

time: 299 us -> 136 us (0.45)
  Pallas kernels: 0 us -> 129 us
  waiting for transfers between devices: 117 us -> 0 us
  starting transfers between devices: 93.6 us -> 0 us
  blocking collectives: 50.9 us -> 0 us
  matrix products: 13.8 us -> 0 us
  other arithmetic: 13.7 us -> 0 us
    pallas_call x0 -> x2, Pallas kernels: none -> 129 us  [the longest x1 126 us: shards(): pl.pallas_call(functools.partial(step_kernel, n_dp, n_tp, dims), out_shap...]
    all_to_all x13 -> x0, waiting for transfers between devices: 117 us -> none  [the longest x2 59.7 us: summed_on_arrival_2(): lax.all_to_all(blocks, axis, split_axis=0, concat_axis=0, tiled=True)]
    all_to_all x13 -> x0, starting transfers between devices: 93.6 us -> none  [the longest x2 50.5 us: summed_on_arrival_2(): lax.all_to_all(blocks, axis, split_axis=0, concat_axis=0, tiled=True)]
    all_to_all x3 -> x0, blocking collectives: 50.9 us -> none  [copy_for_each(): return lax.all_to_all(copies, axis, split_axis=0, concat_axis=0, tiled=True)]
    dot_general x14 -> x0, matrix products: 13.8 us -> none  [the longest x8 11 us: shards(): jnp.dot(scaled_in, weight[blk], preferred_element_type=jnp.float32)]
    reduce_sum x16 -> x0, other arithmetic: 3.96 us -> none  [the longest x2 1.91 us: shards(): squares = jnp.sum(xf * xf, axis=-1)]
    unnamed x48 -> x3, local copies, waits for them, and re-layouts: 0.4 us -> 4.18 us
  transfers between devices with their start and end apart: 13 -> 0, of which waited for: 12 -> 0; matrix products, arithmetic and copies ran while one was open for 9% -> 0% of each run, Pallas kernels for 0% -> 0%
where the time goes in v1:
time: 136 us; the launch traced here: 135 us
  Pallas kernels  129 us (95%)
  local copies, waits for them, and re-layouts  5.54 us (4%)
    pallas_call x1, Pallas kernels, shards(): pl.pallas_call(functools.partial(step_kernel, n_dp, n_tp, dims), out_shap...  126 us
    unnamed x3, local copies, waits for them, and re-layouts  4.18 us
    pallas_call x1, Pallas kernels, shards(): pl.pallas_call(functools.partial(finish_kernel, rows), grid=(blocks,), ou...  3.22 us

profile of v1, /device:TPU:40, one launch (start us, length us, event | category | flops | bytes accessed | tf_op | source)
XLA Modules:
  0.0 135.4 jit_solution(10166236104463683457)
XLA Ops:
  0.6 1.3 copy.17.bias
  1.9 1.4 %copy.18.stab = f32[2,16,1]{2,1,0:T(8,128)} copy(f32[2,16,1]{1,2,0:T(1,128)} %param.23) | data formatting | bytes 256 | tf_op args[11]
  3.3 1.5 %copy.16.gate_w = bf16[2,1,384,2]{3,2,1,0:T(8,128)(2,1)} copy(bf16[2,1,384,2]{2,3,1,0:T(2,128)(2,1)} %param.18) | data formatting | bytes 6144 | tf_op args[6]
  4.8 126.0 %two_cells.1 = (bf16[128,512]{1,0:T(8,128)(2,1)}, f32[2,5,16,128]{3,2,1,0:T(8,128)}) custom-call(bf16[128,512]{1,0:T(8,128)(2,1)} %tokens.1, f32[2,512]{1,0:T(2,128)} %gain.1, bf16[2,512,128]{2,1,0:T(8,128)(2,1)} %wq.1, bf16[2,512,128]{2,1,0:T(8,128)(2,1)} %wk.1, bf16[2,512,128]{2,1,0:T(8,128)(2,1)} %wv.1, bf16[2,512,128]{2,1,0:T(8,128)(2,1)} %wo.1, ...), custom_call_target="tpu_custom_call" | custom-call | tf_op jit(solution)/shard_map/two_cells/pallas_call | solution.py:213
  130.8 3.2 %finish.1 = (bf16[128,512]{1,0:T(8,128)(2,1)}, f32[2,16,1,128,128]{4,3,2,1,0:T(8,128)}, f32[2,16,1,128]{3,2,1,0:T(1,128)}, f32[2,16,1]{2,1,0:T(8,128)}) custom-call(bf16[128,512]{1,0:T(8,128)(2,1)} %get-tuple-element.6.x, f32[2,5,16,128]{3,2,1,0:T(8,128)} %get-tuple-element.7.vec, f32[2,16,1,128,128]{4,3,2,1,0:T(8,128)} %memory.3), custom_call_target="tpu_custom_call" | custom-call | tf_op jit(solution)/shard_map/finish/pallas_call | solution.py:250
  134.0 1.4 %copy.19 = f32[2,16,1]{1,2,0:T(1,128)} copy(f32[2,16,1]{2,1,0:T(8,128)} %get-tuple-element.11) | data formatting | bytes 256 | tf_op jit(solution)/shard_map/finish/pallas_call | solution.py:250

commit v2 on v1

--- a/solution.py
+++ b/solution.py
@@ -19,12 +19,16 @@
     return sorted(range(1, count), key=lambda k: -min(k, count - k))
 
 
+def eye(n):
+    return lax.broadcasted_iota(jnp.int32, (n, n), 0) == lax.broadcasted_iota(jnp.int32, (n, n), 1)
+
+
 def step_kernel(
     n_dp, n_tp, dims,
     tokens, gain, wq, wk, wv, wo, gate_w, bias, wmix, memory, norm, stab,
     x_out, vec_out,
     xbuf, wbuf, mixbuf, membuf, part, send1, recv1, gath, mixpart, send3, recv3, far,
-    load_sem, s1, r1, s2, r2, s3, r3, s4, r4, s5, r5,
+    load_sem, token, s1, r1, s2, r2, s3, r3, s4, r4, s5, r5,
 ):
     blocks, rows, feats, dk, model = dims
     cols = 4 * dk
@@ -45,12 +49,25 @@
     window = [k for k in window if k]
 
     barrier = pltpu.get_barrier_semaphore()
-    peers = [at_tp(NEAR * k) for k in ahead_first(n_far)]
-    peers += [at_near(k) for k in ahead_first(NEAR)]
-    peers += [at_tp(k) for h in range(1, NEAR // 2 + 1) for k in (h, -h)]
-    peers += [at_dp(k) for k in ahead_first(n_dp)]
-    for peer in peers:
-        pl.semaphore_signal(barrier, inc=1, device_id=peer, device_id_type=MESH)
+    circles = [
+        [at_near(k) for k in ahead_first(NEAR)],
+        [at_tp(NEAR * k) for k in ahead_first(n_far)],
+        [at_tp(k) for h in range(1, NEAR // 2 + 1) for k in (h, -h)],
+    ]
+    for k in ahead_first(n_dp):
+        pl.semaphore_signal(barrier, inc=1, device_id=at_dp(k), device_id_type=MESH)
+    lower, higher = jnp.int32(n_dp - 1), []
+    for circle in circles:
+        above = jnp.int32(0)
+        for peer in circle:
+
+            @pl.when(peer["tp"] > tp)
+            def _(peer=peer):
+                pl.semaphore_signal(barrier, inc=1, device_id=peer, device_id_type=MESH)
+
+            above = above + jnp.where(peer["tp"] > tp, 1, 0)
+        lower = lower + (len(circle) - above)
+        higher.append(above)
 
     loads = []
 
@@ -68,7 +85,20 @@
         mem_loads.append(load(memory.at[b, :, 0], membuf.at[b]))
         mix_loads.append(load(wmix.at[b], mixbuf.at[b]))
 
-    pl.semaphore_wait(barrier, len(peers))
+    pl.semaphore_wait(barrier, lower)
+    for i, circle in enumerate(circles):
+        for peer in circle:
+
+            @pl.when(peer["tp"] < tp)
+            def _(peer=peer, i=i):
+                pl.semaphore_signal(token.at[i], inc=1, device_id=peer, device_id_type=MESH)
+
+    def met(b, i):
+        if b == 0:
+
+            @pl.when(higher[i] > 0)
+            def _():
+                pl.semaphore_wait(token.at[i], higher[i])
 
     def rows_of(block):
         return pl.ds(pl.multiple_of(block * rows, rows), rows)
@@ -116,11 +146,13 @@
         query, key, value, outgate = (
             proj[:, i * dk : (i + 1) * dk].astype(jnp.float32) for i in range(4)
         )
-        pre = jnp.dot(proj[:, : 3 * dk], gate_w[b, 0], preferred_element_type=jnp.float32)
+        pre = lax.dot_general(
+            proj[:, : 3 * dk], gate_w[b, 0], (((1,), (1,)), ((), ())), preferred_element_type=jnp.float32
+        )
         log_input = pre[:, 0:1]
-        shifted = pre[:, 1:2] + bias[b : b + 1, 0:1]
+        shifted = pre[:, 1:2] + bias[:, b : b + 1]
         log_forget = jnp.minimum(shifted, 0.0) - jnp.log1p(jnp.exp(-jnp.abs(shifted)))
-        old = stab[b]
+        old = jnp.sum(jnp.where(eye(rows), stab[b], 0.0), axis=1, keepdims=True)
         new_stab = jnp.maximum(log_forget + old, log_input)
         keep = jnp.exp(log_forget + old - new_stab)
         admit = jnp.exp(log_input - new_stab)
@@ -157,6 +189,7 @@
         prod = jnp.dot(gath[b], mixbuf[b], preferred_element_type=jnp.float32)
         mixpart[...] = prod
         send3[b] = prod.astype(jnp.bfloat16)
+        met(b, 0)
         copies = [
             push(send3.at[b, rows_of(lax.rem(j + k, NEAR))], recv3.at[b, k - 1],
                  s3.at[b, k - 1], r3.at[b, k - 1], at_near(k))
@@ -168,6 +201,7 @@
         for k in range(1, NEAR):
             total = total + recv3[b, k - 1].astype(jnp.float32)
         far[b, group] = total.astype(jnp.bfloat16)
+        met(b, 1)
         copies = [
             push(far.at[b, group], far.at[b, group], s4.at[b, k - 1], r4.at[b, k - 1], at_tp(NEAR * k))
             for k in ahead_first(n_far)
@@ -179,6 +213,7 @@
         for k in range(1, n_far):
             mixed = mixed + far[b, k].astype(jnp.float32)
         xbuf[b, rows_of(j), :] = (total + mixed).astype(jnp.bfloat16)
+        met(b, 2)
         copies = [
             push(xbuf.at[b, rows_of(j)], xbuf.at[b, rows_of(j)], s5.at[b, i], r5.at[b, i], at_tp(k))
             for i, k in enumerate(window)
@@ -198,7 +233,7 @@
             + admitted_t[:, s : s + 1] * vec[0, 2, s : s + 1, :]
         )
     norm_out[0, :, 0] = vec[0, 3]
-    stab_out[0] = vec[0, 4, :, 0:1]
+    stab_out[0] = jnp.sum(jnp.where(eye(rows), vec[0, 4, :, :rows], 0.0), axis=0, keepdims=True)
     x_out[...] = x[...]
 
 
@@ -209,6 +244,7 @@
     n_far = n_tp // NEAR
     dims = (blocks, rows, feats, dk, feats * n_dp)
     bf, f32 = jnp.bfloat16, jnp.float32
+    gate_w, bias, stab = gate_w.transpose(0, 1, 3, 2), bias.T, stab.transpose(0, 2, 1)
     dma = pltpu.SemaphoreType.DMA
     x, vec = pl.pallas_call(
         functools.partial(step_kernel, n_dp, n_tp, dims),
@@ -232,6 +268,7 @@
             pltpu.VMEM((blocks, NEAR - 1, rows, feats), bf),
             pltpu.VMEM((blocks, n_far, rows, feats), bf),
             dma((blocks * 6,)),
+            pltpu.SemaphoreType.REGULAR((3,)),
             dma((blocks, n_dp - 1)),
             dma((blocks, n_dp - 1)),
             dma((blocks, n_dp - 1)),
@@ -245,31 +282,30 @@
         ],
         compiler_params=pltpu.CompilerParams(collective_id=0, has_side_effects=True),
         name="two_cells",
-    )(*args)
-    return tuple(
-        pl.pallas_call(
-            functools.partial(finish_kernel, rows),
-            grid=(blocks,),
-            out_shape=(
-                jax.ShapeDtypeStruct((seqs, feats), bf),
-                jax.ShapeDtypeStruct(memory.shape, f32),
-                jax.ShapeDtypeStruct(norm.shape, f32),
-                jax.ShapeDtypeStruct(stab.shape, f32),
-            ),
-            in_specs=[
-                pl.BlockSpec((seqs, feats), lambda b: (0, 0)),
-                pl.BlockSpec((1, 5, rows, dk), lambda b: (b, 0, 0, 0)),
-                pl.BlockSpec((1, rows, 1, dk, dk), lambda b: (b, 0, 0, 0, 0)),
-            ],
-            out_specs=(
-                pl.BlockSpec((seqs, feats), lambda b: (0, 0)),
-                pl.BlockSpec((1, rows, 1, dk, dk), lambda b: (b, 0, 0, 0, 0)),
-                pl.BlockSpec((1, rows, 1, dk), lambda b: (b, 0, 0, 0)),
-                pl.BlockSpec((1, rows, 1), lambda b: (b, 0, 0)),
-            ),
-            name="finish",
-        )(x, vec, memory)
-    )
+    )(tokens, gain, wq, wk, wv, wo, gate_w, bias, wmix, memory, norm, stab)
+    x, new_memory, new_norm, new_stab = pl.pallas_call(
+        functools.partial(finish_kernel, rows),
+        grid=(blocks,),
+        out_shape=(
+            jax.ShapeDtypeStruct((seqs, feats), bf),
+            jax.ShapeDtypeStruct(memory.shape, f32),
+            jax.ShapeDtypeStruct(norm.shape, f32),
+            jax.ShapeDtypeStruct(stab.shape, f32),
+        ),
+        in_specs=[
+            pl.BlockSpec((seqs, feats), lambda b: (0, 0)),
+            pl.BlockSpec((1, 5, rows, dk), lambda b: (b, 0, 0, 0)),
+            pl.BlockSpec((1, rows, 1, dk, dk), lambda b: (b, 0, 0, 0, 0)),
+        ],
+        out_specs=(
+            pl.BlockSpec((seqs, feats), lambda b: (0, 0)),
+            pl.BlockSpec((1, rows, 1, dk, dk), lambda b: (b, 0, 0, 0, 0)),
+            pl.BlockSpec((1, rows, 1, dk), lambda b: (b, 0, 0, 0)),
+            pl.BlockSpec((1, 1, rows), lambda b: (b, 0, 0)),
+        ),
+        name="finish",
+    )(x, vec, memory)
+    return x, new_memory, new_norm, new_stab.transpose(0, 2, 1)
 
 
 def solution(mesh):

time: 136 us -> 131 us (0.963)
  the two profiles are of different devices: /device:TPU:40 before, /device:TPU:34 now
where the time goes in v2:
time: 131 us
  Pallas kernels  130 us (99%)
    pallas_call x1, Pallas kernels, shards(): pl.pallas_call(functools.partial(step_kernel, n_dp, n_tp, dims), out_shap...  127 us
    pallas_call x1, Pallas kernels, shards(): pl.pallas_call(functools.partial(finish_kernel, rows), grid=(blocks,), ou...  3.22 us

profile of v2, /device:TPU:34, one launch (start us, length us, event | category | flops | bytes accessed | tf_op | source)
XLA Modules:
  0.0 130.7 jit_solution(8969579307863164623)
XLA Ops:
  0.6 126.9 %two_cells.1 = (bf16[128,512]{1,0:T(8,128)(2,1)}, f32[2,5,16,128]{3,2,1,0:T(8,128)}) custom-call(bf16[128,512]{1,0:T(8,128)(2,1)} %tokens.1, f32[2,512]{1,0:T(2,128)} %gain.1, bf16[2,512,128]{2,1,0:T(8,128)(2,1)} %wq.1, bf16[2,512,128]{2,1,0:T(8,128)(2,1)} %wk.1, bf16[2,512,128]{2,1,0:T(8,128)(2,1)} %wv.1, bf16[2,512,128]{2,1,0:T(8,128)(2,1)} %wo.1, ...), custom_call_target="tpu_custom_call" | custom-call | tf_op jit(solution)/shard_map/two_cells/pallas_call | solution.py:249
  127.5 3.2 %finish.1 = (bf16[128,512]{1,0:T(8,128)(2,1)}, f32[2,16,1,128,128]{4,3,2,1,0:T(8,128)}, f32[2,16,1,128]{3,2,1,0:T(1,128)}, f32[2,1,16]{2,1,0:T(1,128)}) custom-call(bf16[128,512]{1,0:T(8,128)(2,1)} %get-tuple-element.10.x, f32[2,5,16,128]{3,2,1,0:T(8,128)} %get-tuple-element.11.vec, f32[2,16,1,128,128]{4,3,2,1,0:T(8,128)} %memory.3), custom_call_target="tpu_custom_call" | custom-call | tf_op jit(solution)/shard_map/finish/pallas_call | solution.py:286

commit v3 on v2

--- a/solution.py
+++ b/solution.py
@@ -11,7 +11,7 @@
 MESH = pl.DeviceIdType.MESH
 NEAR = 8
 EXTRA = 128
-ANY = pl.BlockSpec(memory_space=pl.ANY)
+HBM = pl.BlockSpec(memory_space=pltpu.HBM)
 VM = pl.BlockSpec(memory_space=pltpu.VMEM)
 
 
@@ -25,9 +25,9 @@
 
 def step_kernel(
     n_dp, n_tp, dims,
-    tokens, gain, wq, wk, wv, wo, gate_w, bias, wmix, memory, norm, stab,
+    tokens_in, gain_in, wq, wk, wv, wo, gate_in, bias_in, wmix, memory, norm_in, stab_in,
     x_out, vec_out,
-    xbuf, wbuf, mixbuf, membuf, part, send1, recv1, gath, mixpart, send3, recv3, far,
+    tokens, gain, gate_w, bias, norm, stab, xbuf, wbuf, mixbuf, membuf, part, send1, recv1, gath, mixpart, send3, recv3, far,
     load_sem, token, s1, r1, s2, r2, s3, r3, s4, r4, s5, r5,
 ):
     blocks, rows, feats, dk, model = dims
@@ -39,9 +39,6 @@
     def at_dp(k):
         return {"dp": lax.rem(dp + k, n_dp)}
 
-    def at_near(k):
-        return {"tp": group * NEAR + lax.rem(j + k, NEAR)}
-
     def at_tp(k):
         return {"tp": lax.rem(tp + k + n_tp, n_tp)}
 
@@ -50,10 +47,14 @@
 
     barrier = pltpu.get_barrier_semaphore()
     circles = [
-        [at_near(k) for k in ahead_first(NEAR)],
+        [at_tp(k) for h in range(NEAR // 2, 0, -1) for k in (h, -h)],
         [at_tp(NEAR * k) for k in ahead_first(n_far)],
-        [at_tp(k) for h in range(1, NEAR // 2 + 1) for k in (h, -h)],
     ]
+
+    def rank(at):
+        return jnp.where((at == 0) & (dp == 0), n_tp, at)
+
+    own_rank = rank(tp)
     for k in ahead_first(n_dp):
         pl.semaphore_signal(barrier, inc=1, device_id=at_dp(k), device_id_type=MESH)
     lower, higher = jnp.int32(n_dp - 1), []
@@ -61,11 +62,11 @@
         above = jnp.int32(0)
         for peer in circle:
 
-            @pl.when(peer["tp"] > tp)
+            @pl.when(rank(peer["tp"]) > own_rank)
             def _(peer=peer):
                 pl.semaphore_signal(barrier, inc=1, device_id=peer, device_id_type=MESH)
 
-            above = above + jnp.where(peer["tp"] > tp, 1, 0)
+            above = above + jnp.where(rank(peer["tp"]) > own_rank, 1, 0)
         lower = lower + (len(circle) - above)
         higher.append(above)
 
@@ -77,21 +78,27 @@
         loads.append(copy)
         return copy
 
-    w_loads, mix_loads, mem_loads = [], [], []
+    first_loads = [load(tokens_in, tokens), load(gain_in, gain)]
+    w_loads, mix_loads, mem_loads, cell_loads = [], [], [], []
     for b in range(blocks):
         w_loads.append(
             [load(w.at[b], wbuf.at[b, :, pl.ds(i * dk, dk)]) for i, w in enumerate((wq, wk, wv, wo))]
         )
+        if b == 0:
+            small = ((gate_in, gate_w), (bias_in, bias), (norm_in, norm), (stab_in, stab))
+            cell_loads = [load(src, dst) for src, dst in small]
         mem_loads.append(load(memory.at[b, :, 0], membuf.at[b]))
         mix_loads.append(load(wmix.at[b], mixbuf.at[b]))
 
-    pl.semaphore_wait(barrier, lower)
-    for i, circle in enumerate(circles):
-        for peer in circle:
-
-            @pl.when(peer["tp"] < tp)
-            def _(peer=peer, i=i):
-                pl.semaphore_signal(token.at[i], inc=1, device_id=peer, device_id_type=MESH)
+    def enter():
+        with jax.named_scope("wait_barrier"):
+            pl.semaphore_wait(barrier, lower)
+        for i, circle in enumerate(circles):
+            for peer in circle:
+
+                @pl.when(rank(peer["tp"]) < own_rank)
+                def _(peer=peer, i=i):
+                    pl.semaphore_signal(token.at[i], inc=1, device_id=peer, device_id_type=MESH)
 
     def met(b, i):
         if b == 0:
@@ -116,6 +123,8 @@
 
     for b in range(blocks):
         x_now = tokens if b == 0 else xbuf.at[b - 1]
+        for copy in first_loads if b == 0 else ():
+            copy.wait()
         xf = x_now[...].astype(jnp.float32)
         scaled_in = (xf * gain[b : b + 1, :]).astype(jnp.bfloat16)
         squares = jnp.sum(xf * xf, axis=-1, keepdims=True)
@@ -123,11 +132,14 @@
         lane = lax.broadcasted_iota(jnp.int32, (xf.shape[0], EXTRA), 1)
         tail = jnp.where(lane == 0, high, jnp.where(lane == 1, squares - high, 0.0))
         send1[b, :, cols:] = tail.astype(jnp.bfloat16)
-        for copy in w_loads[b]:
-            copy.wait()
+        with jax.named_scope(f"wait_weights_{b}"):
+            for copy in w_loads[b]:
+                copy.wait()
         prod = jnp.dot(scaled_in, wbuf[b], preferred_element_type=jnp.float32)
         part[...] = prod
         send1[b, :, :cols] = prod.astype(jnp.bfloat16)
+        if b == 0:
+            enter()
         copies = [
             push(send1.at[b, rows_of(lax.rem(dp + k, n_dp))], recv1.at[b, k - 1],
                  s1.at[b, k - 1], r1.at[b, k - 1], at_dp(k))
@@ -135,8 +147,9 @@
         ]
         total = part[rows_of(dp), :]
         own_tail = send1[b, rows_of(dp), cols:].astype(jnp.float32)
-        for copy in copies:
-            copy.wait_recv()
+        with jax.named_scope(f"wait_partials_{b}"):
+            for copy in copies:
+                copy.wait_recv()
         for k in range(1, n_dp):
             total = total + recv1[b, k - 1, :, :cols].astype(jnp.float32)
             own_tail = own_tail + recv1[b, k - 1, :, cols:].astype(jnp.float32)
@@ -146,6 +159,8 @@
         query, key, value, outgate = (
             proj[:, i * dk : (i + 1) * dk].astype(jnp.float32) for i in range(4)
         )
+        for copy in cell_loads if b == 0 else ():
+            copy.wait()
         pre = lax.dot_general(
             proj[:, : 3 * dk], gate_w[b, 0], (((1,), (1,)), ((), ())), preferred_element_type=jnp.float32
         )
@@ -184,20 +199,22 @@
         vec_out[b, 3] = new_norm
         vec_out[b, 4] = jnp.broadcast_to(new_stab, (rows, dk))
         mix_loads[b].wait()
-        for copy in copies:
-            copy.wait_recv()
+        with jax.named_scope(f"wait_gated_{b}"):
+            for copy in copies:
+                copy.wait_recv()
         prod = jnp.dot(gath[b], mixbuf[b], preferred_element_type=jnp.float32)
         mixpart[...] = prod
         send3[b] = prod.astype(jnp.bfloat16)
         met(b, 0)
         copies = [
-            push(send3.at[b, rows_of(lax.rem(j + k, NEAR))], recv3.at[b, k - 1],
-                 s3.at[b, k - 1], r3.at[b, k - 1], at_near(k))
-            for k in ahead_first(NEAR)
+            push(send3.at[b, rows_of(lax.rem(tp + k + n_tp, NEAR))], recv3.at[b, i],
+                 s3.at[b, i], r3.at[b, i], at_tp(k))
+            for i, k in enumerate(window)
         ]
         total = mixpart[rows_of(j), :]
-        for copy in copies:
-            copy.wait_recv()
+        with jax.named_scope(f"wait_near_{b}"):
+            for copy in copies:
+                copy.wait_recv()
         for k in range(1, NEAR):
             total = total + recv3[b, k - 1].astype(jnp.float32)
         far[b, group] = total.astype(jnp.bfloat16)
@@ -207,34 +224,68 @@
             for k in ahead_first(n_far)
         ]
         total = x_now[rows_of(j), :].astype(jnp.float32)
-        for copy in copies:
-            copy.wait_recv()
+        with jax.named_scope(f"wait_far_{b}"):
+            for copy in copies:
+                copy.wait_recv()
         mixed = far[b, 0].astype(jnp.float32)
         for k in range(1, n_far):
             mixed = mixed + far[b, k].astype(jnp.float32)
         xbuf[b, rows_of(j), :] = (total + mixed).astype(jnp.bfloat16)
-        met(b, 2)
         copies = [
             push(xbuf.at[b, rows_of(j)], xbuf.at[b, rows_of(j)], s5.at[b, i], r5.at[b, i], at_tp(k))
             for i, k in enumerate(window)
         ]
-        for copy in copies:
-            copy.wait_recv()
+        with jax.named_scope(f"wait_window_{b}"):
+            for copy in copies:
+                copy.wait_recv()
     x_out[...] = xbuf[blocks - 1]
     for copy in sent:
         copy.wait_send()
 
 
-def finish_kernel(rows, x, vec, memory, x_out, mem_out, norm_out, stab_out):
-    admitted_t = vec[0, 1].T
-    for s in range(rows):
-        mem_out[0, s, 0] = (
-            vec[0, 0, s : s + 1, :] * memory[0, s, 0]
-            + admitted_t[:, s : s + 1] * vec[0, 2, s : s + 1, :]
-        )
-    norm_out[0, :, 0] = vec[0, 3]
-    stab_out[0] = jnp.sum(jnp.where(eye(rows), vec[0, 4, :, :rows], 0.0), axis=0, keepdims=True)
-    x_out[...] = x[...]
+def finish_kernel(
+    pieces, x_in, vec_in, memory_in, x_out, mem_out, norm_out, stab_out,
+    x, vec, memory, fresh, new_norm, new_stab, load_sem, store_sem,
+):
+    blocks, rows, _, _ = memory.shape
+    step = rows // pieces
+    loads = [pltpu.make_async_copy(vec_in, vec, load_sem.at[0])]
+    for b in range(blocks):
+        for p in range(pieces):
+            at = pl.ds(p * step, step)
+            loads.append(
+                pltpu.make_async_copy(memory_in.at[b, at, 0], memory.at[b, at], load_sem.at[len(loads)])
+            )
+    loads.append(pltpu.make_async_copy(x_in, x, load_sem.at[len(loads)]))
+    for copy in loads:
+        copy.start()
+    stores = []
+
+    def store(src, dst):
+        copy = pltpu.make_async_copy(src, dst, store_sem.at[len(stores)])
+        copy.start()
+        stores.append(copy)
+
+    loads[0].wait()
+    for b in range(blocks):
+        new_norm[b] = vec[b, 3]
+        new_stab[b] = jnp.sum(jnp.where(eye(rows), vec[b, 4, :, :rows], 0.0), axis=0, keepdims=True)
+        admitted_t = vec[b, 1].T
+        for p in range(pieces):
+            loads[1 + b * pieces + p].wait()
+            for s in range(p * step, (p + 1) * step):
+                fresh[b, s] = (
+                    vec[b, 0, s : s + 1, :] * memory[b, s]
+                    + admitted_t[:, s : s + 1] * vec[b, 2, s : s + 1, :]
+                )
+            at = pl.ds(p * step, step)
+            store(fresh.at[b, at], mem_out.at[b, at, 0])
+    loads[-1].wait()
+    store(x, x_out)
+    store(new_norm, norm_out.at[:, :, 0])
+    store(new_stab, stab_out)
+    for copy in stores:
+        copy.wait()
 
 
 def shards(n_dp, n_tp, *args):
@@ -252,9 +303,10 @@
             jax.ShapeDtypeStruct((seqs, feats), bf),
             jax.ShapeDtypeStruct((blocks, 5, rows, dk), f32),
         ),
-        in_specs=[VM, VM, ANY, ANY, ANY, ANY, VM, VM, ANY, ANY, VM, VM],
+        in_specs=[HBM] * 12,
         out_specs=(VM, VM),
         scratch_shapes=[
+            *(pltpu.VMEM(a.shape, a.dtype) for a in (tokens, gain, gate_w, bias, norm, stab)),
             pltpu.VMEM((blocks, seqs, feats), bf),
             pltpu.VMEM((blocks, feats, 4 * dk), bf),
             pltpu.VMEM((blocks, dk, feats), bf),
@@ -267,8 +319,8 @@
             pltpu.VMEM((blocks, seqs, feats), bf),
             pltpu.VMEM((blocks, NEAR - 1, rows, feats), bf),
             pltpu.VMEM((blocks, n_far, rows, feats), bf),
-            dma((blocks * 6,)),
-            pltpu.SemaphoreType.REGULAR((3,)),
+            dma((blocks * 6 + 6,)),
+            pltpu.SemaphoreType.REGULAR((2,)),
             dma((blocks, n_dp - 1)),
             dma((blocks, n_dp - 1)),
             dma((blocks, n_dp - 1)),
@@ -283,26 +335,28 @@
         compiler_params=pltpu.CompilerParams(collective_id=0, has_side_effects=True),
         name="two_cells",
     )(tokens, gain, wq, wk, wv, wo, gate_w, bias, wmix, memory, norm, stab)
+    pieces = 2
+    copies = blocks * pieces
     x, new_memory, new_norm, new_stab = pl.pallas_call(
-        functools.partial(finish_kernel, rows),
-        grid=(blocks,),
+        functools.partial(finish_kernel, pieces),
         out_shape=(
             jax.ShapeDtypeStruct((seqs, feats), bf),
             jax.ShapeDtypeStruct(memory.shape, f32),
             jax.ShapeDtypeStruct(norm.shape, f32),
             jax.ShapeDtypeStruct(stab.shape, f32),
         ),
-        in_specs=[
-            pl.BlockSpec((seqs, feats), lambda b: (0, 0)),
-            pl.BlockSpec((1, 5, rows, dk), lambda b: (b, 0, 0, 0)),
-            pl.BlockSpec((1, rows, 1, dk, dk), lambda b: (b, 0, 0, 0, 0)),
+        in_specs=[HBM] * 3,
+        out_specs=[HBM] * 4,
+        scratch_shapes=[
+            pltpu.VMEM((seqs, feats), bf),
+            pltpu.VMEM((blocks, 5, rows, dk), f32),
+            pltpu.VMEM((blocks, rows, dk, dk), f32),
+            pltpu.VMEM((blocks, rows, dk, dk), f32),
+            pltpu.VMEM((blocks, rows, dk), f32),
+            pltpu.VMEM((blocks, 1, rows), f32),
+            dma((copies + 2,)),
+            dma((copies + 3,)),
         ],
-        out_specs=(
-            pl.BlockSpec((seqs, feats), lambda b: (0, 0)),
-            pl.BlockSpec((1, rows, 1, dk, dk), lambda b: (b, 0, 0, 0, 0)),
-            pl.BlockSpec((1, rows, 1, dk), lambda b: (b, 0, 0, 0)),
-            pl.BlockSpec((1, 1, rows), lambda b: (b, 0, 0)),
-        ),
         name="finish",
     )(x, vec, memory)
     return x, new_memory, new_norm, new_stab.transpose(0, 2, 1)

time: 131 us -> 117 us (0.89)
  the two profiles are of different devices: /device:TPU:34 before, /device:TPU:40 now
where the time goes in v3:
time: 117 us
  Pallas kernels  116 us (99%)
    pallas_call x1, Pallas kernels, shards(): pl.pallas_call(functools.partial(step_kernel, n_dp, n_tp, dims), out_shap...  114 us
    pallas_call x1, Pallas kernels, shards(): pl.pallas_call(functools.partial(finish_kernel, pieces), out_shape=(jax.S...  2.96 us

profile of v3, /device:TPU:40, one launch (start us, length us, event | category | flops | bytes accessed | tf_op | source)
XLA Modules:
  0.0 117.1 jit_solution(8277914571452472224)
XLA Ops:
  0.6 113.5 %two_cells.1 = (bf16[128,512]{1,0:T(8,128)(2,1)}, f32[2,5,16,128]{3,2,1,0:T(8,128)}) custom-call(bf16[128,512]{1,0:T(8,128)(2,1)} %tokens_in.1, f32[2,512]{1,0:T(2,128)} %gain_in.1, bf16[2,512,128]{2,1,0:T(8,128)(2,1)} %wq.1, bf16[2,512,128]{2,1,0:T(8,128)(2,1)} %wk.1, bf16[2,512,128]{2,1,0:T(8,128)(2,1)} %wv.1, bf16[2,512,128]{2,1,0:T(8,128)(2,1)} %wo.1, ...), custom_call_target="tpu_custom_call" | custom-call | tf_op jit(solution)/shard_map/two_cells/pallas_call | solution.py:300
  114.2 3.0 %finish.1 = (bf16[128,512]{1,0:T(8,128)(2,1)}, f32[2,16,1,128,128]{4,3,2,1,0:T(8,128)}, f32[2,16,1,128]{3,2,1,0:T(1,128)}, f32[2,1,16]{2,1,0:T(1,128)}) custom-call(bf16[128,512]{1,0:T(8,128)(2,1)} %get-tuple-element.10.x_in, f32[2,5,16,128]{3,2,1,0:T(8,128)} %get-tuple-element.11.vec_in, f32[2,16,1,128,128]{4,3,2,1,0:T(8,128)} %memory_in.1), custom_call_target="tpu_custom_call" | custom-call | tf_op jit(solution)/shard_map/finish/pallas_call | solution.py:340

commit v4 on v3

--- a/solution.py
+++ b/solution.py
@@ -27,8 +27,8 @@
     n_dp, n_tp, dims,
     tokens_in, gain_in, wq, wk, wv, wo, gate_in, bias_in, wmix, memory, norm_in, stab_in,
     x_out, vec_out,
-    tokens, gain, gate_w, bias, norm, stab, xbuf, wbuf, mixbuf, membuf, part, send1, recv1, gath, mixpart, send3, recv3, far,
-    load_sem, token, s1, r1, s2, r2, s3, r3, s4, r4, s5, r5,
+    tokens, gain, gate_w, bias, norm, stab, vec, xbuf, wbuf, mixbuf, membuf, part, send1, recv1, gath, mixpart, send3, recv3, far,
+    load_sem, store_sem, token, s1, r1, s2, r2, s3, r3, s4, r4, s5, r5,
 ):
     blocks, rows, feats, dk, model = dims
     cols = 4 * dk
@@ -44,6 +44,21 @@
 
     window = sorted(range(-(NEAR // 2) + 1, NEAR // 2 + 1), key=lambda k: -abs(k))
     window = [k for k in window if k]
+
+    loads = []
+
+    def load(src, dst):
+        copy = pltpu.make_async_copy(src, dst, load_sem.at[len(loads)])
+        copy.start()
+        loads.append(copy)
+        return copy
+
+    def load_weights(b):
+        columns = (wbuf.at[b, :, pl.ds(i * dk, dk)] for i in range(4))
+        return [load(w.at[b], dst) for w, dst in zip((wq, wk, wv, wo), columns)]
+
+    first_loads = [load(tokens_in, tokens), load(gain_in, gain)]
+    w_loads = [load_weights(0)]
 
     barrier = pltpu.get_barrier_semaphore()
     circles = [
@@ -70,23 +85,12 @@
         lower = lower + (len(circle) - above)
         higher.append(above)
 
-    loads = []
-
-    def load(src, dst):
-        copy = pltpu.make_async_copy(src, dst, load_sem.at[len(loads)])
-        copy.start()
-        loads.append(copy)
-        return copy
-
-    first_loads = [load(tokens_in, tokens), load(gain_in, gain)]
-    w_loads, mix_loads, mem_loads, cell_loads = [], [], [], []
+    small = ((gate_in, gate_w), (bias_in, bias), (norm_in, norm), (stab_in, stab))
+    cell_loads = [load(src, dst) for src, dst in small]
+    mem_loads, mix_loads = [], []
     for b in range(blocks):
-        w_loads.append(
-            [load(w.at[b], wbuf.at[b, :, pl.ds(i * dk, dk)]) for i, w in enumerate((wq, wk, wv, wo))]
-        )
-        if b == 0:
-            small = ((gate_in, gate_w), (bias_in, bias), (norm_in, norm), (stab_in, stab))
-            cell_loads = [load(src, dst) for src, dst in small]
+        if b:
+            w_loads.append(load_weights(b))
         mem_loads.append(load(memory.at[b, :, 0], membuf.at[b]))
         mix_loads.append(load(wmix.at[b], mixbuf.at[b]))
 
@@ -110,13 +114,21 @@
     def rows_of(block):
         return pl.ds(pl.multiple_of(block * rows, rows), rows)
 
-    sent = []
-
-    def push(src, dst, send, recv, peer):
-        copy = pltpu.make_async_remote_copy(
+    sent, stores = [], []
+
+    def store(src, dst):
+        copy = pltpu.make_async_copy(src, dst, store_sem.at[len(stores)])
+        copy.start()
+        stores.append(copy)
+
+    def describe(src, dst, send, recv, peer):
+        return pltpu.make_async_remote_copy(
             src_ref=src, dst_ref=dst, send_sem=send, recv_sem=recv,
             device_id=peer, device_id_type=MESH,
         )
+
+    def push(*args):
+        copy = describe(*args)
         copy.start()
         sent.append(copy)
         return copy
@@ -193,11 +205,12 @@
                  s2.at[b, k - 1], r2.at[b, k - 1], at_dp(k))
             for k in ahead_first(n_dp)
         ]
-        vec_out[b, 0] = jnp.broadcast_to(keep, (rows, dk))
-        vec_out[b, 1] = admitted
-        vec_out[b, 2] = value
-        vec_out[b, 3] = new_norm
-        vec_out[b, 4] = jnp.broadcast_to(new_stab, (rows, dk))
+        vec[b, 0] = jnp.broadcast_to(keep, (rows, dk))
+        vec[b, 1] = admitted
+        vec[b, 2] = value
+        vec[b, 3] = new_norm
+        vec[b, 4] = jnp.broadcast_to(new_stab, (rows, dk))
+        store(vec.at[b], vec_out.at[b])
         mix_loads[b].wait()
         with jax.named_scope(f"wait_gated_{b}"):
             for copy in copies:
@@ -219,10 +232,22 @@
             total = total + recv3[b, k - 1].astype(jnp.float32)
         far[b, group] = total.astype(jnp.bfloat16)
         met(b, 1)
-        copies = [
-            push(far.at[b, group], far.at[b, group], s4.at[b, k - 1], r4.at[b, k - 1], at_tp(NEAR * k))
-            for k in ahead_first(n_far)
-        ]
+        last = b == blocks - 1
+        copies, held = [], []
+        for k in ahead_first(n_far):
+            copy = describe(
+                far.at[b, group], far.at[b, group], s4.at[b, k - 1], r4.at[b, k - 1], at_tp(NEAR * k)
+            )
+            copies.append(copy)
+            to = lax.rem(group + k, n_far)
+            inner = (group > 0) & (group < n_far - 1)
+            now = inner | (to == 0) | (to == n_far - 1)
+            if last:
+                held.append((copy, now))
+                pl.when(now)(copy.start)
+            else:
+                copy.start()
+        sent += copies
         total = x_now[rows_of(j), :].astype(jnp.float32)
         with jax.named_scope(f"wait_far_{b}"):
             for copy in copies:
@@ -231,16 +256,22 @@
         for k in range(1, n_far):
             mixed = mixed + far[b, k].astype(jnp.float32)
         xbuf[b, rows_of(j), :] = (total + mixed).astype(jnp.bfloat16)
+        x_next = x_out if last else xbuf.at[b]
         copies = [
-            push(xbuf.at[b, rows_of(j)], xbuf.at[b, rows_of(j)], s5.at[b, i], r5.at[b, i], at_tp(k))
+            push(xbuf.at[b, rows_of(j)], x_next.at[rows_of(j)], s5.at[b, i], r5.at[b, i], at_tp(k))
             for i, k in enumerate(window)
         ]
+        for copy, now in held:
+            pl.when(jnp.logical_not(now))(copy.start)
+        if last:
+            store(xbuf.at[b, rows_of(j)], x_out.at[rows_of(j)])
         with jax.named_scope(f"wait_window_{b}"):
             for copy in copies:
                 copy.wait_recv()
-    x_out[...] = xbuf[blocks - 1]
     for copy in sent:
         copy.wait_send()
+    for copy in stores:
+        copy.wait()
 
 
 def finish_kernel(
@@ -304,9 +335,10 @@
             jax.ShapeDtypeStruct((blocks, 5, rows, dk), f32),
         ),
         in_specs=[HBM] * 12,
-        out_specs=(VM, VM),
+        out_specs=(HBM, HBM),
         scratch_shapes=[
             *(pltpu.VMEM(a.shape, a.dtype) for a in (tokens, gain, gate_w, bias, norm, stab)),
+            pltpu.VMEM((blocks, 5, rows, dk), f32),
             pltpu.VMEM((blocks, seqs, feats), bf),
             pltpu.VMEM((blocks, feats, 4 * dk), bf),
             pltpu.VMEM((blocks, dk, feats), bf),
@@ -320,6 +352,7 @@
             pltpu.VMEM((blocks, NEAR - 1, rows, feats), bf),
             pltpu.VMEM((blocks, n_far, rows, feats), bf),
             dma((blocks * 6 + 6,)),
+            dma((blocks + 1,)),
             pltpu.SemaphoreType.REGULAR((2,)),
             dma((blocks, n_dp - 1)),
             dma((blocks, n_dp - 1)),

time: 117 us -> 117 us (level)
  no operation moved by 1% of the time
where the time goes in v4:
time: 117 us
  Pallas kernels  116 us (99%)
    pallas_call x1, Pallas kernels, shards(): pl.pallas_call(functools.partial(step_kernel, n_dp, n_tp, dims), out_shap...  113 us
    pallas_call x1, Pallas kernels, shards(): pl.pallas_call(functools.partial(finish_kernel, pieces), out_shape=(jax.S...  2.96 us

profile of v4, /device:TPU:40, one launch (start us, length us, event | category | flops | bytes accessed | tf_op | source)
XLA Modules:
  0.0 116.5 jit_solution(88567820208040144)
XLA Ops:
  0.6 112.9 %two_cells.1 = (bf16[128,512]{1,0:T(8,128)(2,1)}, f32[2,5,16,128]{3,2,1,0:T(8,128)}) custom-call(bf16[128,512]{1,0:T(8,128)(2,1)} %tokens_in.1, f32[2,512]{1,0:T(2,128)} %gain_in.1, bf16[2,512,128]{2,1,0:T(8,128)(2,1)} %wq.1, bf16[2,512,128]{2,1,0:T(8,128)(2,1)} %wk.1, bf16[2,512,128]{2,1,0:T(8,128)(2,1)} %wv.1, bf16[2,512,128]{2,1,0:T(8,128)(2,1)} %wo.1, ...), custom_call_target="tpu_custom_call" | custom-call | tf_op jit(solution)/shard_map/two_cells/pallas_call | solution.py:331
  113.6 3.0 %finish.1 = (bf16[128,512]{1,0:T(8,128)(2,1)}, f32[2,16,1,128,128]{4,3,2,1,0:T(8,128)}, f32[2,16,1,128]{3,2,1,0:T(1,128)}, f32[2,1,16]{2,1,0:T(1,128)}) custom-call(bf16[128,512]{1,0:T(8,128)(2,1)} %get-tuple-element.10.x_in, f32[2,5,16,128]{3,2,1,0:T(8,128)} %get-tuple-element.11.vec_in, f32[2,16,1,128,128]{4,3,2,1,0:T(8,128)} %memory_in.1), custom_call_target="tpu_custom_call" | custom-call | tf_op jit(solution)/shard_map/finish/pallas_call | solution.py:373

commit v5 on v4

--- a/solution.py
+++ b/solution.py
@@ -10,7 +10,7 @@
 EPS = 1e-06
 MESH = pl.DeviceIdType.MESH
 NEAR = 8
-EXTRA = 128
+LANES = 128
 HBM = pl.BlockSpec(memory_space=pltpu.HBM)
 VM = pl.BlockSpec(memory_space=pltpu.VMEM)
 
@@ -19,8 +19,9 @@
     return sorted(range(1, count), key=lambda k: -min(k, count - k))
 
 
-def eye(n):
-    return lax.broadcasted_iota(jnp.int32, (n, n), 0) == lax.broadcasted_iota(jnp.int32, (n, n), 1)
+def eye(n, width=None):
+    shape = (n, width or n)
+    return lax.broadcasted_iota(jnp.int32, shape, 0) == lax.broadcasted_iota(jnp.int32, shape, 1)
 
 
 def step_kernel(
@@ -28,7 +29,8 @@
     tokens_in, gain_in, wq, wk, wv, wo, gate_in, bias_in, wmix, memory, norm_in, stab_in,
     x_out, vec_out,
     tokens, gain, gate_w, bias, norm, stab, vec, xbuf, wbuf, mixbuf, membuf, part, send1, recv1, gath, mixpart, send3, recv3, far,
-    load_sem, store_sem, token, s1, r1, s2, r2, s3, r3, s4, r4, s5, r5,
+    squares_out, squares_in, gmix, send6, recv6,
+    load_sem, store_sem, token, s0, r0, s7, r7, s6, r6, s1, r1, s2, r2, s3, r3, s4, r4, s5, r5,
 ):
     blocks, rows, feats, dk, model = dims
     cols = 4 * dk
@@ -92,7 +94,7 @@
         if b:
             w_loads.append(load_weights(b))
         mem_loads.append(load(memory.at[b, :, 0], membuf.at[b]))
-        mix_loads.append(load(wmix.at[b], mixbuf.at[b]))
+        mix_loads.append(load(wmix.at[b], gmix.at[b, dp] if b else mixbuf))
 
     def enter():
         with jax.named_scope("wait_barrier"):
@@ -140,16 +142,16 @@
         xf = x_now[...].astype(jnp.float32)
         scaled_in = (xf * gain[b : b + 1, :]).astype(jnp.bfloat16)
         squares = jnp.sum(xf * xf, axis=-1, keepdims=True)
-        high = squares.astype(jnp.bfloat16).astype(jnp.float32)
-        lane = lax.broadcasted_iota(jnp.int32, (xf.shape[0], EXTRA), 1)
-        tail = jnp.where(lane == 0, high, jnp.where(lane == 1, squares - high, 0.0))
-        send1[b, :, cols:] = tail.astype(jnp.bfloat16)
+        spread = eye(rows, LANES)
+        for k in range(n_dp):
+            own = jnp.where(spread, squares[k * rows : (k + 1) * rows], 0.0)
+            squares_out[b, k] = jnp.sum(own, axis=0, keepdims=True)
         with jax.named_scope(f"wait_weights_{b}"):
             for copy in w_loads[b]:
                 copy.wait()
         prod = jnp.dot(scaled_in, wbuf[b], preferred_element_type=jnp.float32)
         part[...] = prod
-        send1[b, :, :cols] = prod.astype(jnp.bfloat16)
+        send1[b] = prod.astype(jnp.bfloat16)
         if b == 0:
             enter()
         copies = [
@@ -157,15 +159,20 @@
                  s1.at[b, k - 1], r1.at[b, k - 1], at_dp(k))
             for k in ahead_first(n_dp)
         ]
+        copies += [
+            push(squares_out.at[b, lax.rem(dp + k, n_dp)], squares_in.at[b, k - 1],
+                 s0.at[b, k - 1], r0.at[b, k - 1], at_dp(k))
+            for k in ahead_first(n_dp)
+        ]
         total = part[rows_of(dp), :]
-        own_tail = send1[b, rows_of(dp), cols:].astype(jnp.float32)
+        all_squares = squares_out[b, dp]
         with jax.named_scope(f"wait_partials_{b}"):
             for copy in copies:
                 copy.wait_recv()
         for k in range(1, n_dp):
-            total = total + recv1[b, k - 1, :, :cols].astype(jnp.float32)
-            own_tail = own_tail + recv1[b, k - 1, :, cols:].astype(jnp.float32)
-        all_squares = jnp.sum(own_tail, axis=-1, keepdims=True)
+            total = total + recv1[b, k - 1].astype(jnp.float32)
+            all_squares = all_squares + squares_in[b, k - 1]
+        all_squares = jnp.sum(jnp.where(spread, all_squares, 0.0), axis=1, keepdims=True)
         scale = lax.rsqrt(all_squares / model + EPS)
         proj = (scale * total).astype(jnp.bfloat16)
         query, key, value, outgate = (
@@ -199,55 +206,87 @@
         numer = keep * recalled + match * value
         denom = jnp.maximum(jnp.abs(jnp.sum(query * new_norm, axis=-1, keepdims=True)), 1.0)
         gated = numer / denom * jax.nn.sigmoid(outgate)
-        gath[b, rows_of(dp), :] = gated.astype(jnp.bfloat16)
-        copies = [
-            push(gath.at[b, rows_of(dp)], gath.at[b, rows_of(dp)],
-                 s2.at[b, k - 1], r2.at[b, k - 1], at_dp(k))
-            for k in ahead_first(n_dp)
-        ]
+        gated = gated.astype(jnp.bfloat16)
+        if b == 0:
+            gath[rows_of(dp), :] = gated
+            copies = [
+                push(gath.at[rows_of(dp)], gath.at[rows_of(dp)], s2.at[k - 1], r2.at[k - 1], at_dp(k))
+                for k in ahead_first(n_dp)
+            ]
+        else:
+            for copy in mix_copies[b]:
+                copy.wait_recv()
+            turn = lax.rem(dp - tp + n_tp, NEAR)
+            turn = jnp.where(turn > NEAR // 2, turn - NEAR, turn)
+            slot = turn + NEAR // 2 - 1
+            for k in range(n_dp):
+                send6[b, k] = jnp.dot(
+                    gated, gmix[b, k], preferred_element_type=jnp.float32
+                ).astype(jnp.bfloat16)
+            copies = []
+            for k in ahead_first(n_dp):
+                to = lax.rem(dp + k, n_dp)
+                peer = {"dp": to, **at_tp(turn)}
+                push(send6.at[b, to], recv6.at[b, slot], s6.at[b, k], r6.at[b, slot], peer)
+            itself = describe(
+                send6.at[b, dp], recv6.at[b, slot], s6.at[b, 0], r6.at[b, slot], at_tp(turn)
+            )
+            pl.when(turn != 0)(itself.start)
+
+            @pl.when(turn == 0)
+            def _():
+                recv6[b, NEAR // 2 - 1] = send6[b, dp]
         vec[b, 0] = jnp.broadcast_to(keep, (rows, dk))
         vec[b, 1] = admitted
         vec[b, 2] = value
         vec[b, 3] = new_norm
         vec[b, 4] = jnp.broadcast_to(new_stab, (rows, dk))
         store(vec.at[b], vec_out.at[b])
-        mix_loads[b].wait()
-        with jax.named_scope(f"wait_gated_{b}"):
-            for copy in copies:
-                copy.wait_recv()
-        prod = jnp.dot(gath[b], mixbuf[b], preferred_element_type=jnp.float32)
-        mixpart[...] = prod
-        send3[b] = prod.astype(jnp.bfloat16)
-        met(b, 0)
-        copies = [
-            push(send3.at[b, rows_of(lax.rem(tp + k + n_tp, NEAR))], recv3.at[b, i],
-                 s3.at[b, i], r3.at[b, i], at_tp(k))
-            for i, k in enumerate(window)
-        ]
-        total = mixpart[rows_of(j), :]
-        with jax.named_scope(f"wait_near_{b}"):
-            for copy in copies:
-                copy.wait_recv()
-        for k in range(1, NEAR):
-            total = total + recv3[b, k - 1].astype(jnp.float32)
+        if b == 0:
+            mix_loads[b].wait()
+            with jax.named_scope(f"wait_gated_{b}"):
+                for copy in copies:
+                    copy.wait_recv()
+            prod = jnp.dot(gath[...], mixbuf[...], preferred_element_type=jnp.float32)
+            mixpart[...] = prod
+            send3[...] = prod.astype(jnp.bfloat16)
+            met(0, 0)
+            copies = [
+                push(send3.at[rows_of(lax.rem(tp + k + n_tp, NEAR))], recv3.at[i],
+                     s3.at[i], r3.at[i], at_tp(k))
+                for i, k in enumerate(window)
+            ]
+            mix_copies = {}
+            for later in range(1, blocks):
+                mix_loads[later].wait()
+                mix_copies[later] = [
+                    push(gmix.at[later, dp], gmix.at[later, dp],
+                         s7.at[later, k - 1], r7.at[later, k - 1], at_dp(k))
+                    for k in ahead_first(n_dp)
+                ]
+            total = mixpart[rows_of(j), :]
+            with jax.named_scope(f"wait_near_{b}"):
+                for copy in copies:
+                    copy.wait_recv()
+            for i in range(len(window)):
+                total = total + recv3[i].astype(jnp.float32)
+        else:
+            with jax.named_scope(f"wait_near_{b}"):
+                for i in range(NEAR):
+                    arrived = describe(
+                        send6.at[b, 0], recv6.at[b, i], s6.at[b, 0], r6.at[b, i], at_tp(turn)
+                    )
+                    if i == NEAR // 2 - 1:
+                        pl.when(turn != 0)(arrived.wait_recv)
+                    else:
+                        arrived.wait_recv()
+            total = sum(recv6[b, i].astype(jnp.float32) for i in range(NEAR))
         far[b, group] = total.astype(jnp.bfloat16)
         met(b, 1)
-        last = b == blocks - 1
-        copies, held = [], []
-        for k in ahead_first(n_far):
-            copy = describe(
-                far.at[b, group], far.at[b, group], s4.at[b, k - 1], r4.at[b, k - 1], at_tp(NEAR * k)
-            )
-            copies.append(copy)
-            to = lax.rem(group + k, n_far)
-            inner = (group > 0) & (group < n_far - 1)
-            now = inner | (to == 0) | (to == n_far - 1)
-            if last:
-                held.append((copy, now))
-                pl.when(now)(copy.start)
-            else:
-                copy.start()
-        sent += copies
+        copies = [
+            push(far.at[b, group], far.at[b, group], s4.at[b, k - 1], r4.at[b, k - 1], at_tp(NEAR * k))
+            for k in ahead_first(n_far)
+        ]
         total = x_now[rows_of(j), :].astype(jnp.float32)
         with jax.named_scope(f"wait_far_{b}"):
             for copy in copies:
@@ -256,22 +295,26 @@
         for k in range(1, n_far):
             mixed = mixed + far[b, k].astype(jnp.float32)
         xbuf[b, rows_of(j), :] = (total + mixed).astype(jnp.bfloat16)
+        last = b == blocks - 1
         x_next = x_out if last else xbuf.at[b]
         copies = [
             push(xbuf.at[b, rows_of(j)], x_next.at[rows_of(j)], s5.at[b, i], r5.at[b, i], at_tp(k))
             for i, k in enumerate(window)
         ]
-        for copy, now in held:
-            pl.when(jnp.logical_not(now))(copy.start)
         if last:
             store(xbuf.at[b, rows_of(j)], x_out.at[rows_of(j)])
+        if last:
+            for copy in sent[: -len(copies)]:
+                copy.wait_send()
+            pl.when(turn != 0)(itself.wait_send)
+            for copy in stores[:-1]:
+                copy.wait()
         with jax.named_scope(f"wait_window_{b}"):
             for copy in copies:
                 copy.wait_recv()
-    for copy in sent:
+    for copy in copies:
         copy.wait_send()
-    for copy in stores:
-        copy.wait()
+    stores[-1].wait()
 
 
 def finish_kernel(
@@ -341,16 +384,21 @@
             pltpu.VMEM((blocks, 5, rows, dk), f32),
             pltpu.VMEM((blocks, seqs, feats), bf),
             pltpu.VMEM((blocks, feats, 4 * dk), bf),
-            pltpu.VMEM((blocks, dk, feats), bf),
+            pltpu.VMEM((dk, feats), bf),
             pltpu.VMEM((blocks, rows, dk, dk), f32),
             pltpu.VMEM((seqs, 4 * dk), f32),
-            pltpu.VMEM((blocks, seqs, 4 * dk + EXTRA), bf),
-            pltpu.VMEM((blocks, n_dp - 1, rows, 4 * dk + EXTRA), bf),
-            pltpu.VMEM((blocks, seqs, dk), bf),
+            pltpu.VMEM((blocks, seqs, 4 * dk), bf),
+            pltpu.VMEM((blocks, n_dp - 1, rows, 4 * dk), bf),
+            pltpu.VMEM((seqs, dk), bf),
             pltpu.VMEM((seqs, feats), f32),
-            pltpu.VMEM((blocks, seqs, feats), bf),
-            pltpu.VMEM((blocks, NEAR - 1, rows, feats), bf),
+            pltpu.VMEM((seqs, feats), bf),
+            pltpu.VMEM((NEAR - 1, rows, feats), bf),
             pltpu.VMEM((blocks, n_far, rows, feats), bf),
+            pltpu.VMEM((blocks, n_dp, 1, LANES), f32),
+            pltpu.VMEM((blocks, n_dp - 1, 1, LANES), f32),
+            pltpu.VMEM((blocks, n_dp, dk, feats), bf),
+            pltpu.VMEM((blocks, n_dp, rows, feats), bf),
+            pltpu.VMEM((blocks, NEAR, rows, feats), bf),
             dma((blocks * 6 + 6,)),
             dma((blocks + 1,)),
             pltpu.SemaphoreType.REGULAR((2,)),
@@ -358,8 +406,14 @@
             dma((blocks, n_dp - 1)),
             dma((blocks, n_dp - 1)),
             dma((blocks, n_dp - 1)),
-            dma((blocks, NEAR - 1)),
-            dma((blocks, NEAR - 1)),
+            dma((blocks, n_dp)),
+            dma((blocks, NEAR)),
+            dma((blocks, n_dp - 1)),
+            dma((blocks, n_dp - 1)),
+            dma((n_dp - 1,)),
+            dma((n_dp - 1,)),
+            dma((NEAR - 1,)),
+            dma((NEAR - 1,)),
             dma((blocks, n_far - 1)),
             dma((blocks, n_far - 1)),
             dma((blocks, NEAR - 1)),

time: 117 us -> 119 us (1.017)
    pallas_call x1, Pallas kernels: 113 us -> 114 us  [shards(): pl.pallas_call(functools.partial(step_kernel, n_dp, n_tp, dims), out_shap...]
where the time goes in v5:
time: 119 us; the launch traced here: 118 us
  Pallas kernels  117 us (98%)
    pallas_call x1, Pallas kernels, shards(): pl.pallas_call(functools.partial(step_kernel, n_dp, n_tp, dims), out_shap...  114 us
    pallas_call x1, Pallas kernels, shards(): pl.pallas_call(functools.partial(finish_kernel, pieces), out_shape=(jax.S...  2.96 us

profile of v5, /device:TPU:40, one launch (start us, length us, event | category | flops | bytes accessed | tf_op | source)
XLA Modules:
  0.0 118.1 jit_solution(3234259798823225383)
XLA Ops:
  0.6 114.5 %two_cells.1 = (bf16[128,512]{1,0:T(8,128)(2,1)}, f32[2,5,16,128]{3,2,1,0:T(8,128)}) custom-call(bf16[128,512]{1,0:T(8,128)(2,1)} %tokens_in.1, f32[2,512]{1,0:T(2,128)} %gain_in.1, bf16[2,512,128]{2,1,0:T(8,128)(2,1)} %wq.1, bf16[2,512,128]{2,1,0:T(8,128)(2,1)} %wk.1, bf16[2,512,128]{2,1,0:T(8,128)(2,1)} %wv.1, bf16[2,512,128]{2,1,0:T(8,128)(2,1)} %wo.1, ...), custom_call_target="tpu_custom_call" | custom-call | tf_op jit(solution)/shard_map/two_cells/pallas_call | solution.py:374
  115.1 3.0 %finish.1 = (bf16[128,512]{1,0:T(8,128)(2,1)}, f32[2,16,1,128,128]{4,3,2,1,0:T(8,128)}, f32[2,16,1,128]{3,2,1,0:T(1,128)}, f32[2,1,16]{2,1,0:T(1,128)}) custom-call(bf16[128,512]{1,0:T(8,128)(2,1)} %get-tuple-element.10.x_in, f32[2,5,16,128]{3,2,1,0:T(8,128)} %get-tuple-element.11.vec_in, f32[2,16,1,128,128]{4,3,2,1,0:T(8,128)} %memory_in.1), custom_call_target="tpu_custom_call" | custom-call | tf_op jit(solution)/shard_map/finish/pallas_call | solution.py:427

commit v6 on v5

--- a/solution.py
+++ b/solution.py
@@ -208,6 +208,7 @@
         gated = numer / denom * jax.nn.sigmoid(outgate)
         gated = gated.astype(jnp.bfloat16)
         if b == 0:
+            own_block = j
             gath[rows_of(dp), :] = gated
             copies = [
                 push(gath.at[rows_of(dp)], gath.at[rows_of(dp)], s2.at[k - 1], r2.at[k - 1], at_dp(k))
@@ -216,26 +217,30 @@
         else:
             for copy in mix_copies[b]:
                 copy.wait_recv()
-            turn = lax.rem(dp - tp + n_tp, NEAR)
-            turn = jnp.where(turn > NEAR // 2, turn - NEAR, turn)
-            slot = turn + NEAR // 2 - 1
             for k in range(n_dp):
                 send6[b, k] = jnp.dot(
                     gated, gmix[b, k], preferred_element_type=jnp.float32
                 ).astype(jnp.bfloat16)
             copies = []
-            for k in ahead_first(n_dp):
+            for k in (*ahead_first(n_dp), 0):
                 to = lax.rem(dp + k, n_dp)
-                peer = {"dp": to, **at_tp(turn)}
-                push(send6.at[b, to], recv6.at[b, slot], s6.at[b, k], r6.at[b, slot], peer)
-            itself = describe(
-                send6.at[b, dp], recv6.at[b, slot], s6.at[b, 0], r6.at[b, slot], at_tp(turn)
-            )
-            pl.when(turn != 0)(itself.start)
+                turn = lax.rem(dp + to - tp + n_tp, NEAR)
+                turn = jnp.where(turn > NEAR // 2, turn - NEAR, turn)
+                slot = turn + NEAR // 2 - 1
+                copy = describe(
+                    send6.at[b, to], recv6.at[b, slot], s6.at[b, k], r6.at[b, slot],
+                    {"dp": to, **at_tp(turn)},
+                )
+                if k:
+                    copy.start()
+                    sent.append(copy)
+            pl.when(turn != 0)(copy.start)
+            itself = copy
 
             @pl.when(turn == 0)
             def _():
                 recv6[b, NEAR // 2 - 1] = send6[b, dp]
+            own_block = lax.rem(tp - dp + n_dp, NEAR)
         vec[b, 0] = jnp.broadcast_to(keep, (rows, dk))
         vec[b, 1] = admitted
         vec[b, 2] = value
@@ -287,22 +292,22 @@
             push(far.at[b, group], far.at[b, group], s4.at[b, k - 1], r4.at[b, k - 1], at_tp(NEAR * k))
             for k in ahead_first(n_far)
         ]
-        total = x_now[rows_of(j), :].astype(jnp.float32)
+        total = x_now[rows_of(own_block), :].astype(jnp.float32)
         with jax.named_scope(f"wait_far_{b}"):
             for copy in copies:
                 copy.wait_recv()
         mixed = far[b, 0].astype(jnp.float32)
         for k in range(1, n_far):
             mixed = mixed + far[b, k].astype(jnp.float32)
-        xbuf[b, rows_of(j), :] = (total + mixed).astype(jnp.bfloat16)
+        xbuf[b, rows_of(own_block), :] = (total + mixed).astype(jnp.bfloat16)
         last = b == blocks - 1
         x_next = x_out if last else xbuf.at[b]
         copies = [
-            push(xbuf.at[b, rows_of(j)], x_next.at[rows_of(j)], s5.at[b, i], r5.at[b, i], at_tp(k))
+            push(xbuf.at[b, rows_of(own_block)], x_next.at[rows_of(own_block)], s5.at[b, i], r5.at[b, i], at_tp(k))
             for i, k in enumerate(window)
         ]
         if last:
-            store(xbuf.at[b, rows_of(j)], x_out.at[rows_of(j)])
+            store(xbuf.at[b, rows_of(own_block)], x_out.at[rows_of(own_block)])
         if last:
             for copy in sent[: -len(copies)]:
                 copy.wait_send()

time: 119 us -> 115 us (0.966)
  Pallas kernels: 117 us -> 114 us
    pallas_call x1, Pallas kernels: 114 us -> 111 us  [shards(): pl.pallas_call(functools.partial(step_kernel, n_dp, n_tp, dims), out_shap...]
where the time goes in v6:
time: 115 us; the launch traced here: 114 us
  Pallas kernels  114 us (99%)
    pallas_call x1, Pallas kernels, shards(): pl.pallas_call(functools.partial(step_kernel, n_dp, n_tp, dims), out_shap...  111 us
    pallas_call x1, Pallas kernels, shards(): pl.pallas_call(functools.partial(finish_kernel, pieces), out_shape=(jax.S...  2.96 us

profile of v6, /device:TPU:40, one launch (start us, length us, event | category | flops | bytes accessed | tf_op | source)
XLA Modules:
  0.0 114.5 jit_solution(6096366046346524894)
XLA Ops:
  0.6 110.9 %two_cells.1 = (bf16[128,512]{1,0:T(8,128)(2,1)}, f32[2,5,16,128]{3,2,1,0:T(8,128)}) custom-call(bf16[128,512]{1,0:T(8,128)(2,1)} %tokens_in.1, f32[2,512]{1,0:T(2,128)} %gain_in.1, bf16[2,512,128]{2,1,0:T(8,128)(2,1)} %wq.1, bf16[2,512,128]{2,1,0:T(8,128)(2,1)} %wk.1, bf16[2,512,128]{2,1,0:T(8,128)(2,1)} %wv.1, bf16[2,512,128]{2,1,0:T(8,128)(2,1)} %wo.1, ...), custom_call_target="tpu_custom_call" | custom-call | tf_op jit(solution)/shard_map/two_cells/pallas_call | solution.py:379
  111.5 3.0 %finish.1 = (bf16[128,512]{1,0:T(8,128)(2,1)}, f32[2,16,1,128,128]{4,3,2,1,0:T(8,128)}, f32[2,16,1,128]{3,2,1,0:T(1,128)}, f32[2,1,16]{2,1,0:T(1,128)}) custom-call(bf16[128,512]{1,0:T(8,128)(2,1)} %get-tuple-element.10.x_in, f32[2,5,16,128]{3,2,1,0:T(8,128)} %get-tuple-element.11.vec_in, f32[2,16,1,128,128]{4,3,2,1,0:T(8,128)} %memory_in.1), custom_call_target="tpu_custom_call" | custom-call | tf_op jit(solution)/shard_map/finish/pallas_call | solution.py:432

commit v7 on v6

--- a/solution.py
+++ b/solution.py
@@ -30,7 +30,7 @@
     x_out, vec_out,
     tokens, gain, gate_w, bias, norm, stab, vec, xbuf, wbuf, mixbuf, membuf, part, send1, recv1, gath, mixpart, send3, recv3, far,
     squares_out, squares_in, gmix, send6, recv6,
-    load_sem, store_sem, token, s0, r0, s7, r7, s6, r6, s1, r1, s2, r2, s3, r3, s4, r4, s5, r5,
+    load_sem, w_sem, store_sem, token, s0, r0, s7, r7, s6, r6, s1, r1, s2, r2, s3, r3, s4, r4, s5, r5,
 ):
     blocks, rows, feats, dk, model = dims
     cols = 4 * dk
@@ -56,8 +56,9 @@
         return copy
 
     def load_weights(b):
-        columns = (wbuf.at[b, :, pl.ds(i * dk, dk)] for i in range(4))
-        return [load(w.at[b], dst) for w, dst in zip((wq, wk, wv, wo), columns)]
+        for i, w in enumerate((wq, wk, wv, wo)):
+            pltpu.make_async_copy(w.at[b], wbuf.at[b, :, pl.ds(i * dk, dk)], w_sem.at[b]).start()
+        return pltpu.make_async_copy(wbuf.at[b], wbuf.at[b], w_sem.at[b])
 
     first_loads = [load(tokens_in, tokens), load(gain_in, gain)]
     w_loads = [load_weights(0)]
@@ -130,8 +131,10 @@
         )
 
     def push(*args):
-        copy = describe(*args)
-        copy.start()
+        describe(*args).start()
+
+    def all_of(ref, send, recv):
+        copy = describe(ref, ref, send, recv, at_dp(1))
         sent.append(copy)
         return copy
 
@@ -147,23 +150,19 @@
             own = jnp.where(spread, squares[k * rows : (k + 1) * rows], 0.0)
             squares_out[b, k] = jnp.sum(own, axis=0, keepdims=True)
         with jax.named_scope(f"wait_weights_{b}"):
-            for copy in w_loads[b]:
-                copy.wait()
+            w_loads[b].wait()
         prod = jnp.dot(scaled_in, wbuf[b], preferred_element_type=jnp.float32)
         part[...] = prod
         send1[b] = prod.astype(jnp.bfloat16)
         if b == 0:
             enter()
-        copies = [
-            push(send1.at[b, rows_of(lax.rem(dp + k, n_dp))], recv1.at[b, k - 1],
-                 s1.at[b, k - 1], r1.at[b, k - 1], at_dp(k))
-            for k in ahead_first(n_dp)
-        ]
-        copies += [
-            push(squares_out.at[b, lax.rem(dp + k, n_dp)], squares_in.at[b, k - 1],
-                 s0.at[b, k - 1], r0.at[b, k - 1], at_dp(k))
-            for k in ahead_first(n_dp)
-        ]
+        for k in ahead_first(n_dp):
+            to = lax.rem(dp + k, n_dp)
+            push(send1.at[b, rows_of(to)], recv1.at[b, k - 1], s1.at[b], r1.at[b], at_dp(k))
+        for k in ahead_first(n_dp):
+            to = lax.rem(dp + k, n_dp)
+            push(squares_out.at[b, to], squares_in.at[b, k - 1], s0.at[b], r0.at[b], at_dp(k))
+        copies = [all_of(recv1.at[b], s1.at[b], r1.at[b]), all_of(squares_in.at[b], s0.at[b], r0.at[b])]
         total = part[rows_of(dp), :]
         all_squares = squares_out[b, dp]
         with jax.named_scope(f"wait_partials_{b}"):
@@ -210,34 +209,33 @@
         if b == 0:
             own_block = j
             gath[rows_of(dp), :] = gated
-            copies = [
-                push(gath.at[rows_of(dp)], gath.at[rows_of(dp)], s2.at[k - 1], r2.at[k - 1], at_dp(k))
-                for k in ahead_first(n_dp)
-            ]
+            for k in ahead_first(n_dp):
+                push(gath.at[rows_of(dp)], gath.at[rows_of(dp)], s2.at[0], r2.at[0], at_dp(k))
+            copies = [all_of(gath.at[pl.ds(0, (n_dp - 1) * rows)], s2.at[0], r2.at[0])]
         else:
-            for copy in mix_copies[b]:
-                copy.wait_recv()
+            mix_copies[b].wait_recv()
             for k in range(n_dp):
                 send6[b, k] = jnp.dot(
                     gated, gmix[b, k], preferred_element_type=jnp.float32
                 ).astype(jnp.bfloat16)
-            copies = []
             for k in (*ahead_first(n_dp), 0):
                 to = lax.rem(dp + k, n_dp)
                 turn = lax.rem(dp + to - tp + n_tp, NEAR)
                 turn = jnp.where(turn > NEAR // 2, turn - NEAR, turn)
-                slot = turn + NEAR // 2 - 1
                 copy = describe(
-                    send6.at[b, to], recv6.at[b, slot], s6.at[b, k], r6.at[b, slot],
+                    send6.at[b, to], recv6.at[b, turn + NEAR // 2 - 1], s6.at[b], r6.at[b],
                     {"dp": to, **at_tp(turn)},
                 )
                 if k:
                     copy.start()
-                    sent.append(copy)
-            pl.when(turn != 0)(copy.start)
-            itself = copy
-
-            @pl.when(turn == 0)
+                else:
+                    pl.when(turn != 0)(copy.start)
+            stays = turn == 0
+            eight = describe(recv6.at[b], recv6.at[b], s6.at[b], r6.at[b], at_dp(1))
+            seven = recv6.at[b, pl.ds(0, NEAR - 1)]
+            seven = describe(seven, seven, s6.at[b], r6.at[b], at_dp(1))
+
+            @pl.when(stays)
             def _():
                 recv6[b, NEAR // 2 - 1] = send6[b, dp]
             own_block = lax.rem(tp - dp + n_dp, NEAR)
@@ -256,19 +254,18 @@
             mixpart[...] = prod
             send3[...] = prod.astype(jnp.bfloat16)
             met(0, 0)
-            copies = [
-                push(send3.at[rows_of(lax.rem(tp + k + n_tp, NEAR))], recv3.at[i],
-                     s3.at[i], r3.at[i], at_tp(k))
-                for i, k in enumerate(window)
-            ]
+            for i, k in enumerate(window):
+                to = lax.rem(tp + k + n_tp, NEAR)
+                push(send3.at[rows_of(to)], recv3.at[i], s3.at[0], r3.at[0], at_tp(k))
+            copies = [all_of(recv3, s3.at[0], r3.at[0])]
             mix_copies = {}
             for later in range(1, blocks):
                 mix_loads[later].wait()
-                mix_copies[later] = [
-                    push(gmix.at[later, dp], gmix.at[later, dp],
-                         s7.at[later, k - 1], r7.at[later, k - 1], at_dp(k))
-                    for k in ahead_first(n_dp)
-                ]
+                for k in ahead_first(n_dp):
+                    push(gmix.at[later, dp], gmix.at[later, dp], s7.at[later], r7.at[later], at_dp(k))
+                mix_copies[later] = all_of(
+                    gmix.at[later, pl.ds(0, n_dp - 1)], s7.at[later], r7.at[later]
+                )
             total = mixpart[rows_of(j), :]
             with jax.named_scope(f"wait_near_{b}"):
                 for copy in copies:
@@ -277,21 +274,14 @@
                 total = total + recv3[i].astype(jnp.float32)
         else:
             with jax.named_scope(f"wait_near_{b}"):
-                for i in range(NEAR):
-                    arrived = describe(
-                        send6.at[b, 0], recv6.at[b, i], s6.at[b, 0], r6.at[b, i], at_tp(turn)
-                    )
-                    if i == NEAR // 2 - 1:
-                        pl.when(turn != 0)(arrived.wait_recv)
-                    else:
-                        arrived.wait_recv()
+                pl.when(stays)(seven.wait_recv)
+                pl.when(jnp.logical_not(stays))(eight.wait_recv)
             total = sum(recv6[b, i].astype(jnp.float32) for i in range(NEAR))
         far[b, group] = total.astype(jnp.bfloat16)
         met(b, 1)
-        copies = [
-            push(far.at[b, group], far.at[b, group], s4.at[b, k - 1], r4.at[b, k - 1], at_tp(NEAR * k))
-            for k in ahead_first(n_far)
-        ]
+        for k in ahead_first(n_far):
+            push(far.at[b, group], far.at[b, group], s4.at[b], r4.at[b], at_tp(NEAR * k))
+        copies = [all_of(far.at[b, pl.ds(0, n_far - 1)], s4.at[b], r4.at[b])]
         total = x_now[rows_of(own_block), :].astype(jnp.float32)
         with jax.named_scope(f"wait_far_{b}"):
             for copy in copies:
@@ -302,16 +292,17 @@
         xbuf[b, rows_of(own_block), :] = (total + mixed).astype(jnp.bfloat16)
         last = b == blocks - 1
         x_next = x_out if last else xbuf.at[b]
-        copies = [
-            push(xbuf.at[b, rows_of(own_block)], x_next.at[rows_of(own_block)], s5.at[b, i], r5.at[b, i], at_tp(k))
-            for i, k in enumerate(window)
-        ]
+        for k in window:
+            block = rows_of(own_block)
+            push(xbuf.at[b, block], x_next.at[block], s5.at[b], r5.at[b], at_tp(k))
+        copies = [all_of(x_next.at[pl.ds(0, (NEAR - 1) * rows)], s5.at[b], r5.at[b])]
         if last:
             store(xbuf.at[b, rows_of(own_block)], x_out.at[rows_of(own_block)])
         if last:
             for copy in sent[: -len(copies)]:
                 copy.wait_send()
-            pl.when(turn != 0)(itself.wait_send)
+            pl.when(stays)(seven.wait_send)
+            pl.when(jnp.logical_not(stays))(eight.wait_send)
             for copy in stores[:-1]:
                 copy.wait()
         with jax.named_scope(f"wait_window_{b}"):
@@ -404,25 +395,13 @@
             pltpu.VMEM((blocks, n_dp, dk, feats), bf),
             pltpu.VMEM((blocks, n_dp, rows, feats), bf),
             pltpu.VMEM((blocks, NEAR, rows, feats), bf),
-            dma((blocks * 6 + 6,)),
+            dma((blocks * 2 + 6,)),
+            dma((blocks,)),
             dma((blocks + 1,)),
             pltpu.SemaphoreType.REGULAR((2,)),
-            dma((blocks, n_dp - 1)),
-            dma((blocks, n_dp - 1)),
-            dma((blocks, n_dp - 1)),
-            dma((blocks, n_dp - 1)),
-            dma((blocks, n_dp)),
-            dma((blocks, NEAR)),
-            dma((blocks, n_dp - 1)),
-            dma((blocks, n_dp - 1)),
-            dma((n_dp - 1,)),
-            dma((n_dp - 1,)),
-            dma((NEAR - 1,)),
-            dma((NEAR - 1,)),
-            dma((blocks, n_far - 1)),
-            dma((blocks, n_far - 1)),
-            dma((blocks, NEAR - 1)),
-            dma((blocks, NEAR - 1)),
+            *(dma((blocks,)) for _ in range(8)),
+            *(dma((1,)) for _ in range(4)),
+            *(dma((blocks,)) for _ in range(4)),
         ],
         compiler_params=pltpu.CompilerParams(collective_id=0, has_side_effects=True),
         name="two_cells",

time: 115 us -> 113 us (0.983)
  Pallas kernels: 114 us -> 112 us
    pallas_call x1, Pallas kernels: 111 us -> 110 us  [shards(): pl.pallas_call(functools.partial(step_kernel, n_dp, n_tp, dims), out_shap...]
where the time goes in v7:
time: 113 us
  Pallas kernels  112 us (99%)
    pallas_call x1, Pallas kernels, shards(): pl.pallas_call(functools.partial(step_kernel, n_dp, n_tp, dims), out_shap...  110 us
    pallas_call x1, Pallas kernels, shards(): pl.pallas_call(functools.partial(finish_kernel, pieces), out_shape=(jax.S...  2.96 us

profile of v7, /device:TPU:40, one launch (start us, length us, event | category | flops | bytes accessed | tf_op | source)
XLA Modules:
  0.0 113.1 jit_solution(8274418577208682252)
XLA Ops:
  0.6 109.5 %two_cells.1 = (bf16[128,512]{1,0:T(8,128)(2,1)}, f32[2,5,16,128]{3,2,1,0:T(8,128)}) custom-call(bf16[128,512]{1,0:T(8,128)(2,1)} %tokens_in.1, f32[2,512]{1,0:T(2,128)} %gain_in.1, bf16[2,512,128]{2,1,0:T(8,128)(2,1)} %wq.1, bf16[2,512,128]{2,1,0:T(8,128)(2,1)} %wk.1, bf16[2,512,128]{2,1,0:T(8,128)(2,1)} %wv.1, bf16[2,512,128]{2,1,0:T(8,128)(2,1)} %wo.1, ...), custom_call_target="tpu_custom_call" | custom-call | tf_op jit(solution)/shard_map/two_cells/pallas_call | solution.py:370
  110.2 3.0 %finish.1 = (bf16[128,512]{1,0:T(8,128)(2,1)}, f32[2,16,1,128,128]{4,3,2,1,0:T(8,128)}, f32[2,16,1,128]{3,2,1,0:T(1,128)}, f32[2,1,16]{2,1,0:T(1,128)}) custom-call(bf16[128,512]{1,0:T(8,128)(2,1)} %get-tuple-element.10.x_in, f32[2,5,16,128]{3,2,1,0:T(8,128)} %get-tuple-element.11.vec_in, f32[2,16,1,128,128]{4,3,2,1,0:T(8,128)} %memory_in.1), custom_call_target="tpu_custom_call" | custom-call | tf_op jit(solution)/shard_map/finish/pallas_call | solution.py:411

commit v8 on v7

--- a/solution.py
+++ b/solution.py
@@ -144,11 +144,6 @@
             copy.wait()
         xf = x_now[...].astype(jnp.float32)
         scaled_in = (xf * gain[b : b + 1, :]).astype(jnp.bfloat16)
-        squares = jnp.sum(xf * xf, axis=-1, keepdims=True)
-        spread = eye(rows, LANES)
-        for k in range(n_dp):
-            own = jnp.where(spread, squares[k * rows : (k + 1) * rows], 0.0)
-            squares_out[b, k] = jnp.sum(own, axis=0, keepdims=True)
         with jax.named_scope(f"wait_weights_{b}"):
             w_loads[b].wait()
         prod = jnp.dot(scaled_in, wbuf[b], preferred_element_type=jnp.float32)
@@ -159,6 +154,11 @@
         for k in ahead_first(n_dp):
             to = lax.rem(dp + k, n_dp)
             push(send1.at[b, rows_of(to)], recv1.at[b, k - 1], s1.at[b], r1.at[b], at_dp(k))
+        squares = jnp.sum(xf * xf, axis=-1, keepdims=True)
+        spread = eye(rows, LANES)
+        for k in range(n_dp):
+            own = jnp.where(spread, squares[k * rows : (k + 1) * rows], 0.0)
+            squares_out[b, k] = jnp.sum(own, axis=0, keepdims=True)
         for k in ahead_first(n_dp):
             to = lax.rem(dp + k, n_dp)
             push(squares_out.at[b, to], squares_in.at[b, k - 1], s0.at[b], r0.at[b], at_dp(k))
@@ -177,10 +177,19 @@
         query, key, value, outgate = (
             proj[:, i * dk : (i + 1) * dk].astype(jnp.float32) for i in range(4)
         )
+        mem_loads[b].wait()
         for copy in cell_loads if b == 0 else ():
             copy.wait()
         pre = lax.dot_general(
             proj[:, : 3 * dk], gate_w[b, 0], (((1,), (1,)), ((), ())), preferred_element_type=jnp.float32
+        )
+        query_t = query.T
+        recalled = jnp.concatenate(
+            [
+                jnp.sum(query_t[:, s : s + 1] * membuf[b, s], axis=0, keepdims=True)
+                for s in range(rows)
+            ],
+            axis=0,
         )
         log_input = pre[:, 0:1]
         shifted = pre[:, 1:2] + bias[:, b : b + 1]
@@ -192,19 +201,10 @@
         scaled_key = key * dk ** (-0.5)
         admitted = admit * scaled_key
         new_norm = keep * norm[b, :, 0] + admitted
-        mem_loads[b].wait()
-        query_t = query.T
-        recalled = jnp.concatenate(
-            [
-                jnp.sum(query_t[:, s : s + 1] * membuf[b, s], axis=0, keepdims=True)
-                for s in range(rows)
-            ],
-            axis=0,
-        )
         match = jnp.sum(query * admitted, axis=-1, keepdims=True)
         numer = keep * recalled + match * value
         denom = jnp.maximum(jnp.abs(jnp.sum(query * new_norm, axis=-1, keepdims=True)), 1.0)
-        gated = numer / denom * jax.nn.sigmoid(outgate)
+        gated = numer * (1.0 / denom) * jax.nn.sigmoid(outgate)
         gated = gated.astype(jnp.bfloat16)
         if b == 0:
             own_block = j
@@ -258,14 +258,6 @@
                 to = lax.rem(tp + k + n_tp, NEAR)
                 push(send3.at[rows_of(to)], recv3.at[i], s3.at[0], r3.at[0], at_tp(k))
             copies = [all_of(recv3, s3.at[0], r3.at[0])]
-            mix_copies = {}
-            for later in range(1, blocks):
-                mix_loads[later].wait()
-                for k in ahead_first(n_dp):
-                    push(gmix.at[later, dp], gmix.at[later, dp], s7.at[later], r7.at[later], at_dp(k))
-                mix_copies[later] = all_of(
-                    gmix.at[later, pl.ds(0, n_dp - 1)], s7.at[later], r7.at[later]
-                )
             total = mixpart[rows_of(j), :]
             with jax.named_scope(f"wait_near_{b}"):
                 for copy in copies:
@@ -282,6 +274,15 @@
         for k in ahead_first(n_far):
             push(far.at[b, group], far.at[b, group], s4.at[b], r4.at[b], at_tp(NEAR * k))
         copies = [all_of(far.at[b, pl.ds(0, n_far - 1)], s4.at[b], r4.at[b])]
+        if b == 0:
+            mix_copies = {}
+            for later in range(1, blocks):
+                mix_loads[later].wait()
+                for k in ahead_first(n_dp):
+                    push(gmix.at[later, dp], gmix.at[later, dp], s7.at[later], r7.at[later], at_dp(k))
+                mix_copies[later] = all_of(
+                    gmix.at[later, pl.ds(0, n_dp - 1)], s7.at[later], r7.at[later]
+                )
         total = x_now[rows_of(own_block), :].astype(jnp.float32)
         with jax.named_scope(f"wait_far_{b}"):
             for copy in copies:

time: 113 us -> 113 us (level)
  no operation moved by 1% of the time
where the time goes in v8:
time: 113 us; the launch traced here: 112 us
  Pallas kernels  112 us (99%)
    pallas_call x1, Pallas kernels, shards(): pl.pallas_call(functools.partial(step_kernel, n_dp, n_tp, dims), out_shap...  109 us
    pallas_call x1, Pallas kernels, shards(): pl.pallas_call(functools.partial(finish_kernel, pieces), out_shape=(jax.S...  2.96 us

profile of v8, /device:TPU:40, one launch (start us, length us, event | category | flops | bytes accessed | tf_op | source)
XLA Modules:
  0.0 112.4 jit_solution(4214169313629645709)
XLA Ops:
  0.6 108.8 %two_cells.1 = (bf16[128,512]{1,0:T(8,128)(2,1)}, f32[2,5,16,128]{3,2,1,0:T(8,128)}) custom-call(bf16[128,512]{1,0:T(8,128)(2,1)} %tokens_in.1, f32[2,512]{1,0:T(2,128)} %gain_in.1, bf16[2,512,128]{2,1,0:T(8,128)(2,1)} %wq.1, bf16[2,512,128]{2,1,0:T(8,128)(2,1)} %wk.1, bf16[2,512,128]{2,1,0:T(8,128)(2,1)} %wv.1, bf16[2,512,128]{2,1,0:T(8,128)(2,1)} %wo.1, ...), custom_call_target="tpu_custom_call" | custom-call | tf_op jit(solution)/shard_map/two_cells/pallas_call | solution.py:371
  109.5 3.0 %finish.1 = (bf16[128,512]{1,0:T(8,128)(2,1)}, f32[2,16,1,128,128]{4,3,2,1,0:T(8,128)}, f32[2,16,1,128]{3,2,1,0:T(1,128)}, f32[2,1,16]{2,1,0:T(1,128)}) custom-call(bf16[128,512]{1,0:T(8,128)(2,1)} %get-tuple-element.10.x_in, f32[2,5,16,128]{3,2,1,0:T(8,128)} %get-tuple-element.11.vec_in, f32[2,16,1,128,128]{4,3,2,1,0:T(8,128)} %memory_in.1), custom_call_target="tpu_custom_call" | custom-call | tf_op jit(solution)/shard_map/finish/pallas_call | solution.py:412

commit v9 on v8

--- a/solution.py
+++ b/solution.py
@@ -44,8 +44,9 @@
     def at_tp(k):
         return {"tp": lax.rem(tp + k + n_tp, n_tp)}
 
-    window = sorted(range(-(NEAR // 2) + 1, NEAR // 2 + 1), key=lambda k: -abs(k))
+    window = sorted(range(-(NEAR // 2), NEAR // 2), key=lambda k: -abs(k))
     window = [k for k in window if k]
+    other = [-k for k in window]
 
     loads = []
 
@@ -221,9 +222,9 @@
             for k in (*ahead_first(n_dp), 0):
                 to = lax.rem(dp + k, n_dp)
                 turn = lax.rem(dp + to - tp + n_tp, NEAR)
-                turn = jnp.where(turn > NEAR // 2, turn - NEAR, turn)
+                turn = jnp.where(turn >= NEAR // 2, turn - NEAR, turn)
                 copy = describe(
-                    send6.at[b, to], recv6.at[b, turn + NEAR // 2 - 1], s6.at[b], r6.at[b],
+                    send6.at[b, to], recv6.at[b, turn + NEAR // 2], s6.at[b - 1], r6.at[b - 1],
                     {"dp": to, **at_tp(turn)},
                 )
                 if k:
@@ -231,13 +232,13 @@
                 else:
                     pl.when(turn != 0)(copy.start)
             stays = turn == 0
-            eight = describe(recv6.at[b], recv6.at[b], s6.at[b], r6.at[b], at_dp(1))
+            eight = describe(recv6.at[b], recv6.at[b], s6.at[b - 1], r6.at[b - 1], at_dp(1))
             seven = recv6.at[b, pl.ds(0, NEAR - 1)]
-            seven = describe(seven, seven, s6.at[b], r6.at[b], at_dp(1))
+            seven = describe(seven, seven, s6.at[b - 1], r6.at[b - 1], at_dp(1))
 
             @pl.when(stays)
             def _():
-                recv6[b, NEAR // 2 - 1] = send6[b, dp]
+                recv6[b, NEAR // 2] = send6[b, dp]
             own_block = lax.rem(tp - dp + n_dp, NEAR)
         vec[b, 0] = jnp.broadcast_to(keep, (rows, dk))
         vec[b, 1] = admitted
@@ -279,9 +280,9 @@
             for later in range(1, blocks):
                 mix_loads[later].wait()
                 for k in ahead_first(n_dp):
-                    push(gmix.at[later, dp], gmix.at[later, dp], s7.at[later], r7.at[later], at_dp(k))
+                    push(gmix.at[later, dp], gmix.at[later, dp], s7.at[later - 1], r7.at[later - 1], at_dp(k))
                 mix_copies[later] = all_of(
-                    gmix.at[later, pl.ds(0, n_dp - 1)], s7.at[later], r7.at[later]
+                    gmix.at[later, pl.ds(0, n_dp - 1)], s7.at[later - 1], r7.at[later - 1]
                 )
         total = x_now[rows_of(own_block), :].astype(jnp.float32)
         with jax.named_scope(f"wait_far_{b}"):
@@ -293,7 +294,7 @@
         xbuf[b, rows_of(own_block), :] = (total + mixed).astype(jnp.bfloat16)
         last = b == blocks - 1
         x_next = x_out if last else xbuf.at[b]
-        for k in window:
+        for k in (other if last else window):
             block = rows_of(own_block)
             push(xbuf.at[b, block], x_next.at[block], s5.at[b], r5.at[b], at_tp(k))
         copies = [all_of(x_next.at[pl.ds(0, (NEAR - 1) * rows)], s5.at[b], r5.at[b])]
@@ -400,7 +401,9 @@
             dma((blocks,)),
             dma((blocks + 1,)),
             pltpu.SemaphoreType.REGULAR((2,)),
-            *(dma((blocks,)) for _ in range(8)),
+            *(dma((blocks,)) for _ in range(2)),
+            *(dma((blocks - 1,)) for _ in range(4)),
+            *(dma((blocks,)) for _ in range(2)),
             *(dma((1,)) for _ in range(4)),
             *(dma((blocks,)) for _ in range(4)),
         ],

time: 113 us -> 113 us (level)
  no operation moved by 1% of the time
where the time goes in v9:
time: 113 us; the launch traced here: 112 us
  Pallas kernels  112 us (99%)
    pallas_call x1, Pallas kernels, shards(): pl.pallas_call(functools.partial(step_kernel, n_dp, n_tp, dims), out_shap...  109 us
    pallas_call x1, Pallas kernels, shards(): pl.pallas_call(functools.partial(finish_kernel, pieces), out_shape=(jax.S...  2.96 us

profile of v9, /device:TPU:40, one launch (start us, length us, event | category | flops | bytes accessed | tf_op | source)
XLA Modules:
  0.0 112.2 jit_solution(2808961697376484196)
XLA Ops:
  0.6 108.6 %two_cells.1 = (bf16[128,512]{1,0:T(8,128)(2,1)}, f32[2,5,16,128]{3,2,1,0:T(8,128)}) custom-call(bf16[128,512]{1,0:T(8,128)(2,1)} %tokens_in.1, f32[2,512]{1,0:T(2,128)} %gain_in.1, bf16[2,512,128]{2,1,0:T(8,128)(2,1)} %wq.1, bf16[2,512,128]{2,1,0:T(8,128)(2,1)} %wk.1, bf16[2,512,128]{2,1,0:T(8,128)(2,1)} %wv.1, bf16[2,512,128]{2,1,0:T(8,128)(2,1)} %wo.1, ...), custom_call_target="tpu_custom_call" | custom-call | tf_op jit(solution)/shard_map/two_cells/pallas_call | solution.py:372
  109.3 3.0 %finish.1 = (bf16[128,512]{1,0:T(8,128)(2,1)}, f32[2,16,1,128,128]{4,3,2,1,0:T(8,128)}, f32[2,16,1,128]{3,2,1,0:T(1,128)}, f32[2,1,16]{2,1,0:T(1,128)}) custom-call(bf16[128,512]{1,0:T(8,128)(2,1)} %get-tuple-element.10.x_in, f32[2,5,16,128]{3,2,1,0:T(8,128)} %get-tuple-element.11.vec_in, f32[2,16,1,128,128]{4,3,2,1,0:T(8,128)} %memory_in.1), custom_call_target="tpu_custom_call" | custom-call | tf_op jit(solution)/shard_map/finish/pallas_call | solution.py:415
